TPU v7x, 256 devices: a whole 4x4x8 slice. The times are simulated.
256 devices in a mesh: ep: 32 (over z, x), tp: 8 (over y, core).
Axes of the slice: x: 4, y: 4, z: 8, core: 2. Of those that a mesh axis runs over, the one named last changes fastest.
Arguments:
- tokens: bfloat16 [768, 4096], P('ep'), may hold values from -6 to 6
- delta_state: float32 [768, 16, 128, 128], P('ep', 'tp'), may hold values from -0.625 to 0.625
- attn_gain: float32 [4096], replicated, may hold values from 0.1 to 1.9
- query_weight: bfloat16 [4096, 2048], P('ep', 'tp'), may hold values from -0.09375 to 0.09375
- key_weight: bfloat16 [4096, 2048], P('ep', 'tp'), may hold values from -0.09375 to 0.09375
- value_weight: bfloat16 [4096, 2048], P('ep', 'tp'), may hold values from -0.09375 to 0.09375
- decay_weight: bfloat16 [4096, 16], replicated, may hold values from -0.09375 to 0.09375
- beta_weight: bfloat16 [4096, 16], replicated, may hold values from -0.09375 to 0.09375
- decay_rate: float32 [16], P('tp'), may hold values from 0.05 to 3
- head_gain: float32 [128], replicated, may hold values from 0.1 to 1.9
- output_weight: bfloat16 [2048, 4096], P('tp'), may hold values from -0.125 to 0.125
- ffn_gain: float32 [4096], replicated, may hold values from 0.1 to 1.9
- expert_ids: int32 [768, 2], P('ep'), may hold values from 0 to 31, all different within a row; in each aligned block of 24 rows (0 to 23, 24 to 47, ...) at most 3 rows name the same one
- group_prob: float32 [768], P('ep'), may hold values from 0.3 to 1
- expert_logit: float32 [768, 2], P('ep'), may hold values from -8 to 8
- expert_gate: bfloat16 [32, 4096, 1024], P('ep', None, 'tp'), may hold values from -0.09375 to 0.09375
- expert_up: bfloat16 [32, 4096, 1024], P('ep', None, 'tp'), may hold values from -0.09375 to 0.09375
- expert_down: bfloat16 [32, 1024, 4096], P('ep', 'tp'), may hold values from -0.1875 to 0.1875
- dense_gate: bfloat16 [4096, 4096], P('tp', 'ep'), may hold values from -0.09375 to 0.09375
- dense_up: bfloat16 [4096, 4096], P('tp', 'ep'), may hold values from -0.09375 to 0.09375
- dense_down: bfloat16 [4096, 4096], P('ep', 'tp'), may hold values from -0.09375 to 0.09375
- dense_mix: float32 [4096], P('tp'), may hold values from -3 to 3
Outputs:
- mixed_out: bfloat16 [768, 4096], P('ep', 'tp')
- new_state: float32 [768, 16, 128, 128], P('ep', 'tp')
Inputs may be any that keep to these rules, and one draw needn't show every extreme that they name: `expert_ids`: each row names 2 different experts. Among the rows of one device (aligned blocks of 24 rows) no expert is named by more than 3 rows, and in every draw some expert reaches 3 in some block.
All inputs are finite; a program needn't handle non-finite values.
Results may differ from a plain program's by a relative error of at most 0.02.
Values may be sent and summed in bfloat16 or wider, within the bound.
A program may use at most 64 MiB of HBM per device.

v0:
```python
import jax
import jax.numpy as jnp
from jax import lax
from jax.sharding import PartitionSpec as P

EPS = 1e-06


def split_up(shard, dim, count):
    shape = shard.shape
    tiles = shard.reshape(*shape[:dim], count, shape[dim] // count, *shape[dim + 1 :])
    return jnp.moveaxis(tiles, dim, 0)


def summed_on_arrival(shard, axis, dim):
    tiles = split_up(shard, dim, lax.axis_size(axis))
    arrived = lax.all_to_all(tiles, axis, split_axis=0, concat_axis=0, tiled=True)
    return arrived.astype(jnp.float32).sum(axis=0)


def sent_to_all(shard, axis):
    count = lax.axis_size(axis)
    return lax.all_to_all(
        jnp.broadcast_to(shard[None], (count, *shard.shape)), axis, 0, 0, tiled=True
    )


def over_copies(shard, axis):
    everything = sent_to_all(shard, axis)
    return jnp.sum(everything.astype(jnp.float32), axis=0)


def laid_out(tiles, dim):
    shape = list(tiles.shape[1:])
    shape[dim] *= tiles.shape[0]
    return jnp.moveaxis(tiles, 0, dim).reshape(shape)


def collect(shard, axis, dim):
    return laid_out(sent_to_all(shard, axis), dim)


def rms_scale(values, gain):
    mean_sq = jnp.mean(values * values, axis=-1, keepdims=True)
    return values * lax.rsqrt(mean_sq + EPS) * gain


def unit_rows(values):
    return values * lax.rsqrt(jnp.sum(values * values, axis=-1, keepdims=True) + EPS)


def per_device(
    tokens,
    delta_state,
    attn_gain,
    query_weight,
    key_weight,
    value_weight,
    decay_weight,
    beta_weight,
    decay_rate,
    head_gain,
    output_weight,
    ffn_gain,
    expert_ids,
    group_prob,
    expert_logit,
    expert_gate,
    expert_up,
    expert_down,
    dense_gate,
    dense_up,
    dense_down,
    dense_mix,
):
    seq_rows = tokens.shape[0]
    head_count = delta_state.shape[1]
    head_size = delta_state.shape[2]
    width_local = head_count * head_size
    tp_index = lax.axis_index("tp")
    residual = tokens.astype(jnp.float32)
    normed = rms_scale(residual, attn_gain).astype(jnp.bfloat16)
    spread = lax.all_to_all(normed, "ep", split_axis=1, concat_axis=0, tiled=True)
    joined = jnp.concatenate((query_weight, key_weight, value_weight), axis=1)
    summed = summed_on_arrival(
        jnp.dot(spread, joined, preferred_element_type=jnp.float32).astype(jnp.bfloat16), "ep", 0
    )
    query_sum = summed[:, :width_local]
    key_sum = summed[:, width_local : 2 * width_local]
    value_sum = summed[:, 2 * width_local :]

    def heads_of(values):
        rounded = lax.optimization_barrier(values.astype(jnp.bfloat16))
        return rounded.astype(jnp.float32).reshape(seq_rows, head_count, head_size)

    query_unit = unit_rows(heads_of(query_sum)) * head_size ** (-0.5)
    key_unit = unit_rows(heads_of(key_sum))
    value_heads = heads_of(value_sum)
    decay_cols = lax.dynamic_slice_in_dim(decay_weight, tp_index * head_count, head_count, 1)
    beta_cols = lax.dynamic_slice_in_dim(beta_weight, tp_index * head_count, head_count, 1)
    decay_pre = jnp.dot(normed, decay_cols, preferred_element_type=jnp.float32)
    decay = jnp.exp(-decay_rate * jax.nn.softplus(decay_pre))
    beta_gate = jax.nn.sigmoid(jnp.dot(normed, beta_cols, preferred_element_type=jnp.float32))
    recalled = jnp.einsum("bhk,bhkv->bhv", key_unit, delta_state)
    correction = beta_gate[..., None] * (value_heads - decay[..., None] * recalled)
    new_state = (
        decay[..., None, None] * delta_state + key_unit[..., :, None] * correction[..., None, :]
    )
    read_out = jnp.einsum("bhk,bhkv->bhv", query_unit, new_state)
    head_out = rms_scale(read_out, head_gain).astype(jnp.bfloat16).reshape(seq_rows, width_local)
    attn_part = jnp.dot(head_out, output_weight, preferred_element_type=jnp.float32)
    attn_sum = over_copies(attn_part.astype(jnp.bfloat16), "tp").astype(jnp.float32)
    middle = residual + attn_sum
    ffn_in = rms_scale(middle, ffn_gain).astype(jnp.bfloat16)
    slice_width = dense_gate.shape[0]
    hidden_width = dense_gate.shape[1]
    own_columns = lax.dynamic_slice_in_dim(ffn_in, tp_index * slice_width, slice_width, 1)
    gate_up = jnp.concatenate((dense_gate, dense_up), axis=1)
    dense_part = jnp.dot(collect(own_columns, "ep", 0), gate_up, preferred_element_type=jnp.float32)
    dense_sum = over_copies(dense_part.astype(jnp.bfloat16), "tp").astype(jnp.float32)
    dense_hidden = (jax.nn.silu(dense_sum[:, :hidden_width]) * dense_sum[:, hidden_width:]).astype(
        jnp.bfloat16
    )
    dense_out = summed_on_arrival(
        jnp.dot(dense_hidden, dense_down, preferred_element_type=jnp.float32).astype(jnp.bfloat16),
        "ep",
        0,
    )
    expert_count = lax.axis_size("ep")
    top_count = expert_ids.shape[1]
    capacity = max(2, 2 * seq_rows * top_count // expert_count)
    pair_ids = expert_ids.reshape(-1)
    onehot = (pair_ids[:, None] == jnp.arange(expert_count, dtype=jnp.int32)[None, :]).astype(
        jnp.int32
    )
    ranks = jnp.sum(onehot * (jnp.cumsum(onehot, axis=0) - 1), axis=1)
    places = pair_ids * capacity + ranks
    dispatch = (
        jnp.arange(expert_count * capacity, dtype=jnp.int32)[:, None] == places[None, :]
    ).astype(jnp.bfloat16)
    repeated = jnp.repeat(ffn_in, top_count, axis=0)
    outgoing = jnp.dot(dispatch, repeated, preferred_element_type=jnp.float32).astype(jnp.bfloat16)
    outgoing = outgoing.reshape(expert_count, capacity, ffn_in.shape[1])
    arrived = lax.all_to_all(outgoing, "ep", split_axis=0, concat_axis=0, tiled=True)
    gate_vals = jnp.einsum(
        "snd,df->snf", arrived, expert_gate[0], preferred_element_type=jnp.float32
    )
    up_vals = jnp.einsum("snd,df->snf", arrived, expert_up[0], preferred_element_type=jnp.float32)
    expert_hidden = (jax.nn.silu(gate_vals) * up_vals).astype(jnp.bfloat16)
    partial_value = jnp.einsum(
        "snf,fd->snd", expert_hidden, expert_down[0], preferred_element_type=jnp.float32
    )
    summed_cols = summed_on_arrival(partial_value.astype(jnp.bfloat16), "tp", 2)
    returned = lax.all_to_all(
        summed_cols.astype(jnp.bfloat16), "ep", split_axis=0, concat_axis=0, tiled=True
    )
    flat_back = returned.reshape(expert_count * capacity, slice_width)
    picked = (
        jnp.take(flat_back, places, axis=0)
        .astype(jnp.float32)
        .reshape(seq_rows, top_count, slice_width)
    )
    logit_exp = jnp.exp(expert_logit)
    route_weight = group_prob[:, None] * logit_exp / jnp.sum(logit_exp, axis=1, keepdims=True)
    expert_mix = jnp.sum(route_weight[..., None] * picked, axis=1)
    own_middle = lax.dynamic_slice_in_dim(middle, tp_index * slice_width, slice_width, 1)
    mixed_out = (own_middle + jax.nn.sigmoid(dense_mix) * dense_out + expert_mix).astype(
        jnp.bfloat16
    )
    return (mixed_out, new_state)


def solution(mesh):
    return jax.shard_map(
        per_device,
        mesh=mesh,
        in_specs=(
            P("ep", None),
            P("ep", "tp", None, None),
            P(),
            P("ep", "tp"),
            P("ep", "tp"),
            P("ep", "tp"),
            P(),
            P(),
            P("tp"),
            P(),
            P("tp", None),
            P(),
            P("ep", None),
            P("ep"),
            P("ep", None),
            P("ep", None, "tp"),
            P("ep", None, "tp"),
            P("ep", "tp", None),
            P("tp", "ep"),
            P("tp", "ep"),
            P("ep", "tp"),
            P("tp"),
        ),
        out_specs=(P("ep", "tp"), P("ep", "tp", None, None)),
        check_vma=False,
    )
```

profile of v0, /device:TPU:2, one launch (start us, length us, event | category | flops | bytes accessed | tf_op | source)
XLA Modules:
  0.0 269.3 jit_solution(17994246620742949373)
XLA Ops:
  0.7 1.2 fusion.12
  1.9 1.1 copy_bitcast_fusion
  3.0 21.2 %all_to_all.59 = bf16[24,32,128]{2,0,1:T(8,128)(2,1)S(1)} all-to-all(bf16[24,32,128]{2,0,1:T(8,128)(2,1)S(1)} %copy_bitcast_fusion), channel_id=1, replica_groups=mesh['ep'=32,'tp'=8] {'ep'}, dimensions={1} | all-to-all | bytes 393216 | tf_op jit(solution)/shard_map/all_to_all | solution.py:83
  24.2 2.4 convolution_convert_fusion.3
  26.6 5.7 %all-to-all-start.1 = ((bf16[32,24,768]{2,1,0:T(8,128)(2,1)}), bf16[32,24,768]{2,1,0:T(8,128)(2,1)S(1)}, u32[]{:S(2)}, u32[]{:S(2)}) async-start(bf16[32,24,768]{2,1,0:T(8,128)(2,1)} %bitcast.60), calls=%async_computation.1 | async-start | bytes 2359296 | tf_op jit(solution)/shard_map/all_to_all | solution.py:17
  32.3 1.1 fusion.40
  33.5 1.1 fusion.3
  34.6 0.1 copy.116
  34.7 27.5 %all-to-all-done.1 = bf16[32,24,768]{2,1,0:T(8,128)(2,1)S(1)} async-done(((bf16[32,24,768]{2,1,0:T(8,128)(2,1)}), bf16[32,24,768]{2,1,0:T(8,128)(2,1)S(1)}, u32[]{:S(2)}, u32[]{:S(2)}) %all-to-all-start.1) | async-done | bytes 1179680 | tf_op jit(solution)/shard_map/all_to_all | solution.py:17
  62.2 0.2 reduce.1
  62.4 0.1 multiply_reduce_fusion.4
  62.6 0.1 multiply_multiply_fusion
  62.7 0.1 multiply_reduce_fusion.3
  62.8 0.1 broadcast_multiply_fusion
  62.9 2.6 fusion.54
  65.5 0.1 subtract_multiply_fusion
  65.6 1.1 multiply_add_fusion
  66.8 1.6 copy-done.2
  68.4 0.5 fusion.55
  68.9 0.1 multiply_reduce_fusion.2
  69.1 0.1 multiply_convert_fusion.1
  69.2 0.4 convolution_convert_fusion.2
  69.6 1.3 broadcast_in_dim.15
  70.9 4.6 %all-to-all-start.2 = ((bf16[8,24,4096]{2,1,0:T(8,128)(2,1)}), bf16[8,24,4096]{2,1,0:T(8,128)(2,1)}, u32[]{:S(2)}, u32[]{:S(2)}) async-start(bf16[8,24,4096]{2,1,0:T(8,128)(2,1)} %broadcast_in_dim.15), calls=%async_computation.2 | async-start | bytes 3145728 | tf_op jit(solution)/shard_map/all_to_all | solution.py:23
  75.6 0.1 reshape.169
  75.8 0.2 select_reduce_fusion
  76.0 21.1 %all-to-all-done.2 = bf16[8,24,4096]{2,1,0:T(8,128)(2,1)} async-done(((bf16[8,24,4096]{2,1,0:T(8,128)(2,1)}), bf16[8,24,4096]{2,1,0:T(8,128)(2,1)}, u32[]{:S(2)}, u32[]{:S(2)}) %all-to-all-start.2) | async-done | bytes 1572896 | tf_op jit(solution)/shard_map/all_to_all | solution.py:23
  97.2 1.7 convert_reduce_fusion.1
  98.8 0.2 multiply_reduce_fusion
  99.0 0.1 multiply_convert_fusion
  99.1 0.3 broadcast_in_dim.19
  99.5 0.3 copy-done.5
  99.8 0.9 reshape.170
  100.7 1.3 convolution_convert_fusion.1
  102.0 1.3 reshape.171
  103.3 5.6 %all-to-all-start.6 = ((bf16[32,3,4096]{2,1,0:T(4,128)(2,1)}), bf16[32,3,4096]{2,1,0:T(4,128)(2,1)S(1)}, u32[]{:S(2)}, u32[]{:S(2)}) async-start(bf16[32,3,4096]{2,1,0:T(4,128)(2,1)} %reshape.171), calls=%async_computation.6 | async-start | bytes 2097152 | tf_op jit(solution)/shard_map/all_to_all | solution.py:144
  108.9 1.4 constant_dynamic-slice_fusion
  110.3 26.4 %all-to-all-done.6 = bf16[32,3,4096]{2,1,0:T(4,128)(2,1)S(1)} async-done(((bf16[32,3,4096]{2,1,0:T(4,128)(2,1)}), bf16[32,3,4096]{2,1,0:T(4,128)(2,1)S(1)}, u32[]{:S(2)}, u32[]{:S(2)}) %all-to-all-start.6) | async-done | bytes 786464 | tf_op jit(solution)/shard_map/all_to_all | solution.py:144
  136.7 1.7 broadcast_in_dim.16
  138.4 5.6 %all-to-all-start.3 = ((bf16[32,24,512]{2,1,0:T(8,128)(2,1)}), bf16[32,24,512]{2,1,0:T(8,128)(2,1)}, u32[]{:S(2)}, u32[]{:S(2)}) async-start(bf16[32,24,512]{2,1,0:T(8,128)(2,1)} %broadcast_in_dim.16), calls=%async_computation.3 | async-start | bytes 1572864 | tf_op jit(solution)/shard_map/all_to_all | solution.py:23
  144.0 2.6 fusion.7
  146.6 3.6 %convolution_convert_fusion = bf16[32,3,4096]{2,0,1:T(8,128)(2,1)} fusion(bf16[1,128,4096]{2,1,0:T(8,128)(2,1)} %param.39, bf16[1,4096,128]{2,1,0:T(8,128)(2,1)} %param.38, bf16[32,3,4096]{2,1,0:T(4,128)(2,1)S(1)} %all-to-all-done.6, f32[32,3,128]{2,0,1:T(8,128)} %fusion.7), kind=kOutput, calls=%fused_computation.2 | convolution fusion | flops 201793536 | bytes 3719168 | tf_op jit(solution)/shard_map/snf,fd->snd/dot_general | solution.py:150
  150.2 2.2 copy.150
  152.3 12.9 %all-to-all-done.3 = bf16[32,24,512]{2,1,0:T(8,128)(2,1)} async-done(((bf16[32,24,512]{2,1,0:T(8,128)(2,1)}), bf16[32,24,512]{2,1,0:T(8,128)(2,1)}, u32[]{:S(2)}, u32[]{:S(2)}) %all-to-all-start.3) | async-done | bytes 786464 | tf_op jit(solution)/shard_map/all_to_all | solution.py:23
  165.2 3.5 %all-to-all-start.7 = ((bf16[8,32,3,512]{3,1,2,0:T(8,128)(2,1)}), bf16[8,32,3,512]{3,1,2,0:T(8,128)(2,1)S(1)}, u32[]{:S(2)}, u32[]{:S(2)}) async-start(bf16[8,32,3,512]{3,1,2,0:T(8,128)(2,1)} %bitcast.62), calls=%async_computation.7 | async-start | bytes 1572864 | tf_op jit(solution)/shard_map/all_to_all | solution.py:17
  168.8 2.2 convolution_convert_fusion.5
  171.1 10.8 %all-to-all-done.7 = bf16[8,32,3,512]{3,1,2,0:T(8,128)(2,1)S(1)} async-done(((bf16[8,32,3,512]{3,1,2,0:T(8,128)(2,1)}), bf16[8,32,3,512]{3,1,2,0:T(8,128)(2,1)S(1)}, u32[]{:S(2)}, u32[]{:S(2)}) %all-to-all-start.7) | async-done | bytes 786464 | tf_op jit(solution)/shard_map/all_to_all | solution.py:17
  181.8 2.9 %broadcast_in_dim.17 = bf16[8,768,256]{2,1,0:T(8,128)(2,1)} broadcast(bf16[768,256]{1,0:T(8,128)(2,1)} %convolution_convert_fusion.5), dimensions={1,2} | broadcast | bytes 3538944 | tf_op jit(solution)/shard_map/broadcast_in_dim | solution.py:24
  184.7 4.4 %all-to-all-start.4 = ((bf16[8,768,256]{2,1,0:T(8,128)(2,1)}), bf16[8,768,256]{2,1,0:T(8,128)(2,1)}, u32[]{:S(2)}, u32[]{:S(2)}) async-start(bf16[8,768,256]{2,1,0:T(8,128)(2,1)} %broadcast_in_dim.17), calls=%async_computation.4 | async-start | bytes 6291456 | tf_op jit(solution)/shard_map/all_to_all | solution.py:23
  189.2 0.1 reduce_sum.136
  189.3 0.7 copy.128
  190.0 37.5 %all-to-all-done.4 = bf16[8,768,256]{2,1,0:T(8,128)(2,1)} async-done(((bf16[8,768,256]{2,1,0:T(8,128)(2,1)}), bf16[8,768,256]{2,1,0:T(8,128)(2,1)}, u32[]{:S(2)}, u32[]{:S(2)}) %all-to-all-start.4) | async-done | bytes 3145760 | tf_op jit(solution)/shard_map/all_to_all | solution.py:23
  227.6 5.6 %all-to-all-start.8 = ((bf16[32,3,512]{2,1,0:T(4,128)(2,1)}), bf16[32,3,512]{2,1,0:T(4,128)(2,1)S(1)}, u32[]{:S(2)}, u32[]{:S(2)}) async-start(bf16[32,3,512]{2,1,0:T(4,128)(2,1)} %copy.128), calls=%async_computation.8 | async-start | bytes 262144 | tf_op jit(solution)/shard_map/all_to_all | solution.py:154
  233.2 2.4 convert_reduce_fusion
  235.6 1.3 convolution_convert_fusion.4
  236.8 5.2 %all-to-all-done.8 = bf16[32,3,512]{2,1,0:T(4,128)(2,1)S(1)} async-done(((bf16[32,3,512]{2,1,0:T(4,128)(2,1)}), bf16[32,3,512]{2,1,0:T(4,128)(2,1)S(1)}, u32[]{:S(2)}, u32[]{:S(2)}) %all-to-all-start.8) | async-done | bytes 98336 | tf_op jit(solution)/shard_map/all_to_all | solution.py:154
  242.0 5.5 %all-to-all-start.5 = ((bf16[32,24,512]{2,1,0:T(8,128)(2,1)}), bf16[32,24,512]{2,1,0:T(8,128)(2,1)S(1)}, u32[]{:S(2)}, u32[]{:S(2)}) async-start(bf16[32,24,512]{2,1,0:T(8,128)(2,1)} %bitcast.64), calls=%async_computation.5 | async-start | bytes 1572864 | tf_op jit(solution)/shard_map/all_to_all | solution.py:17
  247.7 0.1 mul.260
  247.9 0.1 copy.123
  248.2 0.7 gather_fusion
  248.9 0.2 multiply_reduce_fusion.1
  249.2 19.4 %all-to-all-done.5 = bf16[32,24,512]{2,1,0:T(8,128)(2,1)S(1)} async-done(((bf16[32,24,512]{2,1,0:T(8,128)(2,1)}), bf16[32,24,512]{2,1,0:T(8,128)(2,1)S(1)}, u32[]{:S(2)}, u32[]{:S(2)}) %all-to-all-start.5) | async-done | bytes 786464 | tf_op jit(solution)/shard_map/all_to_all | solution.py:17
  268.6 0.1 convert_reduce_fusion.2
  268.7 0.6 add_convert_fusion
  (60 shorter events, 1.0 us)
Async XLA Ops:
  0.6 68.5 %copy-start = (bf16[256,4096]{1,0:T(8,128)(2,1)S(1)}, bf16[256,4096]{1,0:T(8,128)(2,1)}, u32[]{:S(2)}) copy-start(bf16[256,4096]{1,0:T(8,128)(2,1)} %param.32) | copy-start | bytes 6291460
  0.6 31.6 %copy-start.3 = (bf16[24,4096]{1,0:T(8,128)(2,1)S(1)}, bf16[24,4096]{1,0:T(8,128)(2,1)}, u32[]{:S(2)}) copy-start(bf16[24,4096]{1,0:T(8,128)(2,1)} %param.22) | copy-start | bytes 589828
  0.7 31.6 %copy-start.6 = (f32[4096]{0:T(1024)S(1)}, f32[4096]{0:T(1024)}, u32[]{:S(2)}) copy-start(f32[4096]{0:T(1024)} %param.24) | copy-start | bytes 49156
  0.7 31.6 %copy-start.16 = (f32[2]{0:T(128)S(1)}, f32[2]{0:T(128)}, u32[]{:S(2)}) copy-start(f32[2]{0:T(128)} %param.30) | copy-start | bytes 28
  26.6 35.7 %all-to-all-start.1 = ((bf16[32,24,768]{2,1,0:T(8,128)(2,1)}), bf16[32,24,768]{2,1,0:T(8,128)(2,1)S(1)}, u32[]{:S(2)}, u32[]{:S(2)}) async-start(bf16[32,24,768]{2,1,0:T(8,128)(2,1)} %bitcast.60), calls=%async_computation.1 | async-start | bytes 2359296 | tf_op jit(solution)/shard_map/all_to_all | solution.py:17
  62.7 2.9 %copy-start.1 = (f32[24,2,128,128]{3,2,1,0:T(8,128)S(1)}, f32[24,2,128,128]{3,2,1,0:T(8,128)}, u32[]{:S(2)}) copy-start(f32[24,2,128,128]{3,2,1,0:T(8,128)} %param.23) | copy-start | bytes 9437188
  66.7 1.7 copy-start.2
  66.7 2.3 copy-start.11
  69.2 6.3 %copy-start.8 = (s32[24,2]{0,1:T(2,128)S(1)}, s32[24,2]{0,1:T(2,128)}, u32[]{:S(2)}) copy-start(s32[24,2]{0,1:T(2,128)} %param.34) | copy-start | bytes 580
  69.6 29.3 %copy-start.4 = (bf16[24,4096]{1,0:T(8,128)(2,1)S(1)}, bf16[24,4096]{1,0:T(8,128)(2,1)}, u32[]{:S(2)}) copy-start(bf16[24,4096]{1,0:T(8,128)(2,1)} %param.22) | copy-start | bytes 589828
  70.9 28.1 %copy-start.7 = (f32[4096]{0:T(1024)S(1)}, f32[4096]{0:T(1024)}, u32[]{:S(2)}) copy-start(f32[4096]{0:T(1024)} %param.33) | copy-start | bytes 49156
  70.9 26.3 %all-to-all-start.2 = ((bf16[8,24,4096]{2,1,0:T(8,128)(2,1)}), bf16[8,24,4096]{2,1,0:T(8,128)(2,1)}, u32[]{:S(2)}, u32[]{:S(2)}) async-start(bf16[8,24,4096]{2,1,0:T(8,128)(2,1)} %broadcast_in_dim.15), calls=%async_computation.2 | async-start | bytes 3145728 | tf_op jit(solution)/shard_map/all_to_all | solution.py:23
  99.1 0.7 copy-start.5
  103.3 33.3 %all-to-all-start.6 = ((bf16[32,3,4096]{2,1,0:T(4,128)(2,1)}), bf16[32,3,4096]{2,1,0:T(4,128)(2,1)S(1)}, u32[]{:S(2)}, u32[]{:S(2)}) async-start(bf16[32,3,4096]{2,1,0:T(4,128)(2,1)} %reshape.171), calls=%async_computation.6 | async-start | bytes 2097152 | tf_op jit(solution)/shard_map/all_to_all | solution.py:144
  138.4 26.9 %all-to-all-start.3 = ((bf16[32,24,512]{2,1,0:T(8,128)(2,1)}), bf16[32,24,512]{2,1,0:T(8,128)(2,1)}, u32[]{:S(2)}, u32[]{:S(2)}) async-start(bf16[32,24,512]{2,1,0:T(8,128)(2,1)} %broadcast_in_dim.16), calls=%async_computation.3 | async-start | bytes 1572864 | tf_op jit(solution)/shard_map/all_to_all | solution.py:23
  150.2 18.6 %copy-start.13 = (bf16[512,128]{1,0:T(8,128)(2,1)S(1)}, bf16[512,128]{1,0:T(8,128)(2,1)}, u32[]{:S(2)}) copy-start(bf16[512,128]{1,0:T(8,128)(2,1)} %param.41) | copy-start | bytes 393220
  150.2 18.6 %copy-start.14 = (bf16[512,128]{1,0:T(8,128)(2,1)S(1)}, bf16[512,128]{1,0:T(8,128)(2,1)}, u32[]{:S(2)}) copy-start(bf16[512,128]{1,0:T(8,128)(2,1)} %param.40) | copy-start | bytes 393220
  165.2 16.6 %all-to-all-start.7 = ((bf16[8,32,3,512]{3,1,2,0:T(8,128)(2,1)}), bf16[8,32,3,512]{3,1,2,0:T(8,128)(2,1)S(1)}, u32[]{:S(2)}, u32[]{:S(2)}) async-start(bf16[8,32,3,512]{3,1,2,0:T(8,128)(2,1)} %bitcast.62), calls=%async_computation.7 | async-start | bytes 1572864 | tf_op jit(solution)/shard_map/all_to_all | solution.py:17
  184.7 42.9 %all-to-all-start.4 = ((bf16[8,768,256]{2,1,0:T(8,128)(2,1)}), bf16[8,768,256]{2,1,0:T(8,128)(2,1)}, u32[]{:S(2)}, u32[]{:S(2)}) async-start(bf16[8,768,256]{2,1,0:T(8,128)(2,1)} %broadcast_in_dim.17), calls=%async_computation.4 | async-start | bytes 6291456 | tf_op jit(solution)/shard_map/all_to_all | solution.py:23
  189.3 46.3 %copy-start.15 = (bf16[128,512]{1,0:T(8,128)(2,1)S(1)}, bf16[128,512]{1,0:T(8,128)(2,1)}, u32[]{:S(2)}) copy-start(bf16[128,512]{1,0:T(8,128)(2,1)} %param.42) | copy-start | bytes 393220
  227.6 14.4 %all-to-all-start.8 = ((bf16[32,3,512]{2,1,0:T(4,128)(2,1)}), bf16[32,3,512]{2,1,0:T(4,128)(2,1)S(1)}, u32[]{:S(2)}, u32[]{:S(2)}) async-start(bf16[32,3,512]{2,1,0:T(4,128)(2,1)} %copy.128), calls=%async_computation.8 | async-start | bytes 262144 | tf_op jit(solution)/shard_map/all_to_all | solution.py:154
  233.1 14.8 %copy-start.10 = (f32[24,2]{0,1:T(2,128)S(1)}, f32[24,2]{0,1:T(2,128)}, u32[]{:S(2)}) copy-start(f32[24,2]{0,1:T(2,128)} %param.36) | copy-start | bytes 580
  233.1 14.9 %copy-start.12 = (f32[24]{0:T(128)S(1)}, f32[24]{0:T(128)}, u32[]{:S(2)}) copy-start(f32[24]{0:T(128)} %param.35) | copy-start | bytes 292
  233.2 15.0 %copy-start.9 = (f32[512]{0:T(512)S(1)}, f32[512]{0:T(512)}, u32[]{:S(2)}) copy-start(f32[512]{0:T(512)} %param.43) | copy-start | bytes 6148
  242.0 26.6 %all-to-all-start.5 = ((bf16[32,24,512]{2,1,0:T(8,128)(2,1)}), bf16[32,24,512]{2,1,0:T(8,128)(2,1)S(1)}, u32[]{:S(2)}, u32[]{:S(2)}) async-start(bf16[32,24,512]{2,1,0:T(8,128)(2,1)} %bitcast.64), calls=%async_computation.5 | async-start | bytes 1572864 | tf_op jit(solution)/shard_map/all_to_all | solution.py:17
where the time goes:
time: 271 us; the launch traced here: 269 us
  waiting for transfers between devices  161 us (59%)
  starting transfers between devices  40.5 us (15%)
  blocking collectives  21.2 us (8%)
  matrix products  19.1 us (7%)
  local copies, waits for them, and re-layouts  16.5 us (6%)
  other arithmetic  10.1 us (4%)
    all_to_all x3, waiting for transfers between devices, sent_to_all(): lax.all_to_all(jnp.broadcast_to(shard[None], (count, *shard.shape)), axis...  71.6 us
    all_to_all x3, waiting for transfers between devices, summed_on_arrival(): lax.all_to_all(tiles, axis, split_axis=0, concat_axis=0, tiled=True)  57.7 us
    all_to_all x1, waiting for transfers between devices, per_device(): lax.all_to_all(outgoing, 'ep', split_axis=0, concat_axis=0, tiled=True)  26.4 us
    all_to_all x1, blocking collectives, per_device(): lax.all_to_all(normed, 'ep', split_axis=1, concat_axis=0, tiled=True)  21.2 us
    all_to_all x3, starting transfers between devices, summed_on_arrival(): lax.all_to_all(tiles, axis, split_axis=0, concat_axis=0, tiled=True)  14.7 us
    all_to_all x3, starting transfers between devices, sent_to_all(): lax.all_to_all(jnp.broadcast_to(shard[None], (count, *shard.shape)), axis...  14.7 us
    broadcast_in_dim x3, local copies, waits for them, and re-layouts, sent_to_all(): jnp.broadcast_to(shard[None], (count, *shard.shape))  5.88 us
    all_to_all x1, starting transfers between devices, per_device(): lax.all_to_all(summed_cols.astype(jnp.bfloat16), 'ep', split_axis=0, conc...  5.56 us
  transfers between devices with their start and end apart: 8, of which 8 were waited for; matrix products, arithmetic and copies ran while one was open for 8% of the time, Pallas kernels for 0%

commit v1 on v0

v1 whole, which is shorter than its diff:
```python
import jax
import jax.numpy as jnp
from jax import lax
from jax.experimental import pallas as pl
from jax.experimental.pallas import tpu as pltpu
from jax.sharding import PartitionSpec as P

EPS = 1e-06
MESH = pl.DeviceIdType.MESH
F32 = jnp.float32
BF16 = jnp.bfloat16

NX, NZ, NT = 4, 8, 8
ROWS = 24
D = 4096
SL = 512
HEAD = 128
CAP = 3
SLOTS = NZ * CAP


def kernel(
    tok_h, state_h, again_h, wq_h, wk_h, wv_h, dT_h, bT_h, rate_s, hgain_h, wo_h, fgain_h, info_h,
    eg_h, eu_h, ed_h, dg_h, du_h, dd_h, mix_h,
    out_ref, state_o,
    tok, tokf, again, wqkv, db, hgain, wo, fgain, info, wgu, wdn, mixv, egu, edn, state,
    spread, act, psrc, pdst, rout, asrc, adst, ssb, xall, dsrc, ddst, hall, esrc, eall, ehall, rsrc, rdst, fsrc, fdst,
    lsem, xs, xr, zs, zr, ts, tr,
):
    ep = lax.axis_index("ep")
    tp = lax.axis_index("tp")
    z = ep // NX
    x = lax.rem(ep, NX)

    def at_x(d):
        return {"ep": z * NX + lax.rem(x + d, NX), "tp": tp}

    def at_z(d):
        return {"ep": lax.rem(z + d, NZ) * NX + x, "tp": tp}

    def at_t(d):
        return {"ep": ep, "tp": lax.rem(tp + d, NT)}

    def remote(src, dst, ss, rs, dev):
        return pltpu.make_async_remote_copy(
            src_ref=src, dst_ref=dst, send_sem=ss, recv_sem=rs, device_id=dev, device_id_type=MESH
        )

    sent = []

    def go(copy):
        copy.start()
        sent.append(copy)
        return copy

    local = []

    def load(src, dst):
        c = pltpu.make_async_copy(src, dst, lsem.at[len(local)])
        c.start()
        local.append(c)
        return c

    l_tok = load(tok_h, tok)
    l_again = load(again_h, again)
    l_w = [load(w, wqkv.at[m, x]) for m, w in enumerate((wk_h, wv_h, wq_h))]
    l_info = load(info_h, info)
    l_db = [load(dT_h, db.at[0]), load(bT_h, db.at[1])]
    l_gu = [load(dg_h, wgu.at[x, :, pl.ds(0, 128)]), load(du_h, wgu.at[x, :, pl.ds(128, 128)])]
    l_dn = load(dd_h, wdn.at[x])
    l_ed = load(ed_h.at[:, pl.ds(pl.multiple_of(tp * SL, SL), SL)], edn.at[tp])
    l_state = load(state_h, state)
    l_wo = load(wo_h, wo)
    l_small = [
        load(hgain_h, hgain),
        load(fgain_h.at[:, pl.ds(pl.multiple_of(tp * SL, SL), SL)], fgain),
        load(mix_h, mixv),
        load(tok_h.at[:, pl.ds(pl.multiple_of(tp * SL, SL), SL)], tokf),
    ]
    l_egu = [load(eg_h, egu.at[:, pl.ds(0, 128)]), load(eu_h, egu.at[:, pl.ds(128, 128)])]

    bar = pltpu.get_barrier_semaphore()
    for d in range(1, NX):
        pl.semaphore_signal(bar, inc=1, device_id=at_x(d), device_id_type=MESH)
    for d in range(1, NZ):
        pl.semaphore_signal(bar, inc=1, device_id=at_z(d), device_id_type=MESH)
    for d in range(1, NT):
        pl.semaphore_signal(bar, inc=1, device_id=at_t(d), device_id_type=MESH)

    l_tok.wait()
    l_again.wait()
    t32 = tok[...].astype(F32)
    ms = jnp.sum(t32 * t32, axis=1, keepdims=True) * (1.0 / D)
    normed = (t32 * lax.rsqrt(ms + EPS) * again[...]).astype(BF16)
    for b in range(NZ):
        spread[b] = normed[:, b * SL : (b + 1) * SL]

    pl.semaphore_wait(bar, NX + NZ + NT - 3)

    nsx = [0]
    nsz = [0]
    nst = [0]

    def nx():
        nsx[0] += 1
        return nsx[0] - 1

    def nz():
        nsz[0] += 1
        return nsz[0] - 1

    def nt():
        nst[0] += 1
        return nst[0] - 1

    left = lax.rem(x + NX - 1, NX)
    right = lax.rem(x + 1, NX)

    def gather_start(buf):
        a, b = nx(), nx()
        c0 = go(remote(buf.at[x], buf.at[x], xs.at[a], xr.at[a], at_x(1)))
        c1 = go(remote(buf.at[x], buf.at[x], xs.at[b], xr.at[b], at_x(NX - 1)))
        return c0, c1

    def gather_relay(buf, c0, c1):
        h = buf.shape[1] // 2
        a, b = nx(), nx()
        c0.wait_recv()
        r0 = go(remote(
            buf.at[left, pl.ds(0, h)], buf.at[left, pl.ds(0, h)], xs.at[a], xr.at[a], at_x(1)))
        c1.wait_recv()
        r1 = go(remote(
            buf.at[right, pl.ds(h, h)], buf.at[right, pl.ds(h, h)], xs.at[b], xr.at[b], at_x(NX - 1)))
        return r0, r1

    for c in l_w:
        c.wait()
    g_w = [gather_start(wqkv.at[m]) for m in range(3)]

    c_spread = []
    for d in range(1, NZ):
        i = nz()
        zd = lax.rem(z + d, NZ)
        c_spread.append(go(remote(spread.at[zd], act.at[z], zs.at[i], zr.at[i], at_z(d))))
    act[z] = spread[z]

    c_ed = []
    for d in range(1, NT):
        i = nt()
        td = lax.rem(tp + d, NT)
        c_ed.append(go(remote(
            ed_h.at[:, pl.ds(pl.multiple_of(td * SL, SL), SL)], edn.at[tp], ts.at[i], tr.at[i], at_t(d))))

    for c in l_db:
        c.wait()
    dims = (((1,), (1,)), ((), ()))
    dpre = lax.dot_general(normed, db[0], dims, preferred_element_type=F32)
    bpre = lax.dot_general(normed, db[1], dims, preferred_element_type=F32)
    lane16 = lax.broadcasted_iota(jnp.int32, dpre.shape, 1)
    decay, beta = [], []
    for h in range(2):
        pick = lane16 == tp * 2 + h
        dp = jnp.sum(jnp.where(pick, dpre, 0.0), axis=1, keepdims=True)
        bp = jnp.sum(jnp.where(pick, bpre, 0.0), axis=1, keepdims=True)
        soft = jnp.maximum(dp, 0.0) + jnp.log(1.0 + jnp.exp(-jnp.abs(dp)))
        decay.append(jnp.exp(-rate_s[h] * soft))
        beta.append(1.0 / (1.0 + jnp.exp(-bp)))

    l_info.wait()
    inf = info[...]
    id0, id1 = inf[:, 0:1], inf[:, 1:2]
    e0, e1 = jnp.exp(inf[:, 2:3]), jnp.exp(inf[:, 3:4])
    den = e0 + e1
    w0, w1 = inf[:, 4:5] * e0 / den, inf[:, 4:5] * e1 / den
    lanef = lax.broadcasted_iota(jnp.int32, (ROWS, 128), 1).astype(F32)
    rowi = lax.broadcasted_iota(jnp.int32, (ROWS, 128), 0)
    oh = jnp.where((lanef == id0) | (lanef == id1), 1.0, 0.0)
    rank = jnp.zeros((ROWS, 128), F32)
    for i in range(ROWS - 1):
        rank = rank + jnp.where(rowi > i, oh[i : i + 1, :], 0.0)
    table = (rank + 1.0) * oh
    for idk, wk in ((id0, w0), (id1, w1)):
        whi = wk.astype(BF16).astype(F32)
        table = table + jnp.where(lanef == idk + 32.0, whi, 0.0)
        table = table + jnp.where(lanef == idk + 64.0, wk - whi, 0.0)
    rout[z] = table.astype(BF16)

    r_w = [gather_relay(wqkv.at[m], *g_w[m]) for m in range(3)]

    for c in c_spread:
        c.wait_recv()
    acts = act[...].reshape(NZ * ROWS, SL)
    c_p = []
    for m in range(3):
        for c in r_w[m]:
            c.wait_recv()
        part = jnp.dot(acts, wqkv[m].reshape(SL, 2 * HEAD), preferred_element_type=F32)
        psrc[m] = part.astype(BF16).reshape(NZ, ROWS, 2 * HEAD)
        row = []
        for d in range(1, NZ):
            i = nz()
            zd = lax.rem(z + d, NZ)
            row.append(go(remote(psrc.at[m, zd], pdst.at[m, z], zs.at[i], zr.at[i], at_z(d))))
        pdst[m, z] = psrc[m, z]
        c_p.append(row)

    c_r = []
    for d in range(1, NZ):
        i = nz()
        c_r.append(go(remote(rout.at[z], rout.at[z], zs.at[i], zr.at[i], at_z(d))))
    for c in l_gu:
        c.wait()
    l_dn.wait()
    g_gu = gather_start(wgu)
    g_dn = gather_start(wdn)

    qkv = []
    for m in range(3):
        for c in c_p[m]:
            c.wait_recv()
        s = pdst[m, 0].astype(F32)
        for b in range(1, NZ):
            s = s + pdst[m, b].astype(F32)
        qkv.append(s.astype(BF16).astype(F32))
    kk, vv, qq = qkv

    l_state.wait()
    for c in l_small:
        c.wait()
    heads = []
    for h in range(2):
        sl = slice(h * HEAD, (h + 1) * HEAD)
        kh, vh, qh = kk[:, sl], vv[:, sl], qq[:, sl]
        ku = kh * lax.rsqrt(jnp.sum(kh * kh, axis=1, keepdims=True) + EPS)
        qu = qh * lax.rsqrt(jnp.sum(qh * qh, axis=1, keepdims=True) + EPS) * HEAD ** (-0.5)
        kT = ku.T
        qT = qu.T
        kq = jnp.sum(ku * qu, axis=1, keepdims=True)
        rec, red = [], []
        for b in range(ROWS):
            st = state[b, h]
            rec.append(jnp.sum(st * kT[:, b : b + 1], axis=0, keepdims=True))
            red.append(jnp.sum(st * qT[:, b : b + 1], axis=0, keepdims=True))
        rec = jnp.concatenate(rec, axis=0)
        red = jnp.concatenate(red, axis=0)
        corr = beta[h] * (vh - decay[h] * rec)
        ro = decay[h] * red + kq * corr
        ro = ro * lax.rsqrt(jnp.mean(ro * ro, axis=1, keepdims=True) + EPS) * hgain[...]
        heads.append(ro.astype(BF16))
        qkv[h] = (kT, corr)

    l_wo.wait()
    hcat = jnp.concatenate(heads, axis=1)
    for t in range(NT):
        asrc[t] = jnp.dot(hcat, wo[:, t * SL : (t + 1) * SL], preferred_element_type=F32).astype(BF16)
    c_a = []
    for d in range(1, NT):
        i = nt()
        td = lax.rem(tp + d, NT)
        c_a.append(go(remote(asrc.at[td], adst.at[tp], ts.at[i], tr.at[i], at_t(d))))
    adst[tp] = asrc[tp]

    for h in range(2):
        kT, corr = qkv[h]
        dcol = decay[h]
        for b in range(ROWS):
            state_o[b, h] = state[b, h] * dcol[b : b + 1, :] + kT[:, b : b + 1] * corr[b : b + 1, :]

    for c in c_a:
        c.wait_recv()
    asum = adst[0].astype(F32)
    for b in range(1, NT):
        asum = asum + adst[b].astype(F32)
    middle = tokf[...].astype(F32) + asum
    ss = jnp.sum(middle * middle, axis=1, keepdims=True)
    eye = lax.broadcasted_iota(jnp.int32, (ROWS, 128), 0) == lax.broadcasted_iota(jnp.int32, (ROWS, 128), 1)
    ssb[tp] = jnp.sum(jnp.where(eye, ss, 0.0), axis=0, keepdims=True)
    c_s = []
    for d in range(1, NT):
        i = nt()
        c_s.append(go(remote(ssb.at[tp], ssb.at[tp], ts.at[i], tr.at[i], at_t(d))))
    r_gu = gather_relay(wgu, *g_gu)
    r_dn = gather_relay(wdn, *g_dn)
    for c in c_s:
        c.wait_recv()
    srow = ssb[0]
    for b in range(1, NT):
        srow = srow + ssb[b]
    scol = jnp.sum(jnp.where(eye, jnp.broadcast_to(srow, (ROWS, 128)), 0.0), axis=1, keepdims=True)
    ffn = (middle * lax.rsqrt(scol * (1.0 / D) + EPS) * fgain[...]).astype(BF16)
    xall[z] = ffn
    c_x = []
    for d in range(1, NZ):
        i = nz()
        c_x.append(go(remote(xall.at[z], xall.at[z], zs.at[i], zr.at[i], at_z(d))))

    for c in c_r:
        c.wait_recv()
    rt = rout[...].astype(F32)
    shape3 = (NZ, ROWS, 128)
    lane3 = lax.broadcasted_iota(jnp.int32, shape3, 2)
    blk3 = lax.broadcasted_iota(jnp.int32, shape3, 0)
    sel = jnp.zeros(shape3, F32)
    hi = jnp.zeros(shape3, F32)
    lo = jnp.zeros(shape3, F32)
    for xx in range(NX):
        e = z * NX + xx
        r = jnp.sum(jnp.where(lane3 == e, rt, 0.0), axis=2, keepdims=True)
        wh = jnp.sum(jnp.where(lane3 == e + 32, rt, 0.0), axis=2, keepdims=True)
        wl = jnp.sum(jnp.where(lane3 == e + 64, rt, 0.0), axis=2, keepdims=True)
        place = blk3.astype(F32) * CAP + (r - 1.0) + float(xx * SLOTS)
        hit = (lane3.astype(F32) == place) & (r > 0.5)
        sel = sel + jnp.where(hit, 1.0, 0.0)
        hi = hi + jnp.where(hit, wh, 0.0)
        lo = lo + jnp.where(hit, wl, 0.0)
    ntok = NZ * ROWS
    selT = sel.reshape(ntok, 128).T.astype(BF16)
    hi2 = hi.reshape(ntok, 128).astype(BF16)
    lo2 = lo.reshape(ntok, 128).astype(BF16)

    for c in c_x:
        c.wait_recv()
    xs2 = xall[...].reshape(ntok, SL)
    picked = jnp.dot(selT, xs2, preferred_element_type=F32).astype(BF16)
    for xx in range(NX):
        esrc[xx] = picked[xx * SLOTS : (xx + 1) * SLOTS]
    c_e = []
    for d in range(1, NX):
        i = nx()
        xd = lax.rem(x + d, NX)
        c_e.append(go(remote(esrc.at[xd], eall.at[tp, x], xs.at[i], xr.at[i], at_x(d))))
    eall[tp, x] = esrc[x]

    for c in r_gu:
        c.wait_recv()
    for xx in range(NX):
        part = jnp.dot(xs2, wgu[xx], preferred_element_type=F32).astype(BF16)
        dsrc[:, :, xx * 256 : (xx + 1) * 256] = part.reshape(NZ, ROWS, 256)

    for c in c_e:
        c.wait_recv()
    c_ea = []
    for d in range(1, NT):
        i = nt()
        c_ea.append(go(remote(eall.at[tp], eall.at[tp], ts.at[i], tr.at[i], at_t(d))))
    c_d = []
    for d in range(1, NT):
        i = nt()
        td = lax.rem(tp + d, NT)
        c_d.append(go(remote(dsrc.at[td], ddst.at[tp], ts.at[i], tr.at[i], at_t(d))))
    ddst[tp] = dsrc[tp]

    for c in l_egu:
        c.wait()
    for c in c_ea:
        c.wait_recv()
    acc = jnp.zeros((NX * SLOTS, 256), F32)
    for t in range(NT):
        acc = acc + jnp.dot(
            eall[t].reshape(NX * SLOTS, SL), egu[t * SL : (t + 1) * SL, :], preferred_element_type=F32)
    ga, ua = acc[:, :128], acc[:, 128:]
    ehall[tp] = (ga / (1.0 + jnp.exp(-ga)) * ua).astype(BF16)
    c_eh = []
    for d in range(1, NT):
        i = nt()
        c_eh.append(go(remote(ehall.at[tp], ehall.at[tp], ts.at[i], tr.at[i], at_t(d))))

    for c in c_d:
        c.wait_recv()
    dsum = ddst[0].astype(F32)
    for b in range(1, NT):
        dsum = dsum + ddst[b].astype(F32)
    hid = []
    for xx in range(NX):
        g = dsum[:, xx * 256 : xx * 256 + 128]
        u = dsum[:, xx * 256 + 128 : xx * 256 + 256]
        hid.append((g / (1.0 + jnp.exp(-g)) * u).astype(BF16))
    hall[tp] = jnp.concatenate(hid, axis=1)
    c_h = []
    for d in range(1, NT):
        i = nt()
        c_h.append(go(remote(hall.at[tp], hall.at[tp], ts.at[i], tr.at[i], at_t(d))))

    l_ed.wait()
    for c in c_ed:
        c.wait_recv()
    for c in c_eh:
        c.wait_recv()
    eres = jnp.zeros((NX * SLOTS, SL), F32)
    for t in range(NT):
        eres = eres + jnp.dot(ehall[t], edn[t], preferred_element_type=F32)
    rsrc[...] = eres.astype(BF16).reshape(NX, SLOTS, SL)
    c_b = []
    for d in range(1, NX):
        i = nx()
        xd = lax.rem(x + d, NX)
        c_b.append(go(remote(rsrc.at[xd], rdst.at[x], xs.at[i], xr.at[i], at_x(d))))
    rdst[x] = rsrc[x]

    for c in r_dn:
        c.wait_recv()
    for c in c_h:
        c.wait_recv()
    down = jnp.dot(
        hall[...].reshape(ntok, SL), wdn[...].reshape(SL, SL), preferred_element_type=F32)
    down = down * (1.0 / (1.0 + jnp.exp(-mixv[...])))
    for c in c_b:
        c.wait_recv()
    back = rdst[...].reshape(NX * SLOTS, SL)
    down = down + jnp.dot(hi2[:, : NX * SLOTS], back, preferred_element_type=F32)
    down = down + jnp.dot(lo2[:, : NX * SLOTS], back, preferred_element_type=F32)
    fsrc[...] = down.astype(BF16).reshape(NZ, ROWS, SL)
    c_f = []
    for d in range(1, NZ):
        i = nz()
        zd = lax.rem(z + d, NZ)
        c_f.append(go(remote(fsrc.at[zd], fdst.at[z], zs.at[i], zr.at[i], at_z(d))))
    fdst[z] = fsrc[z]
    for c in c_f:
        c.wait_recv()
    total = middle
    for b in range(NZ):
        total = total + fdst[b].astype(F32)
    out_ref[...] = total.astype(BF16)

    for c in sent:
        c.wait_send()


def per_device(
    tokens, delta_state, attn_gain, query_weight, key_weight, value_weight, decay_weight, beta_weight, decay_rate,
    head_gain, output_weight, ffn_gain, expert_ids, group_prob, expert_logit, expert_gate, expert_up, expert_down,
    dense_gate, dense_up, dense_down, dense_mix,
):
    info = jnp.concatenate(
        (
            expert_ids.astype(F32),
            expert_logit,
            group_prob[:, None],
            jnp.zeros((ROWS, 123), F32),
        ),
        axis=1,
    )
    anyspec = pl.BlockSpec(memory_space=pl.ANY)
    in_specs = [anyspec] * 20
    in_specs[8] = pl.BlockSpec(memory_space=pltpu.SMEM)
    vm = pltpu.VMEM
    scratch = [
        vm((ROWS, D), BF16), vm((ROWS, SL), BF16), vm((1, D), F32), vm((3, NX, 128, 256), BF16), vm((2, 16, D), BF16),
        vm((1, HEAD), F32), vm((256, D), BF16), vm((1, SL), F32), vm((ROWS, 128), F32),
        vm((NX, SL, 256), BF16), vm((NX, 128, SL), BF16), vm((1, SL), F32), vm((D, 256), BF16), vm((NT, 128, SL), BF16),
        vm((ROWS, 2, HEAD, HEAD), F32),
        vm((NZ, ROWS, SL), BF16), vm((NZ, ROWS, SL), BF16),
        vm((3, NZ, ROWS, 256), BF16), vm((3, NZ, ROWS, 256), BF16), vm((NZ, ROWS, 128), BF16),
        vm((NT, ROWS, SL), BF16), vm((NT, ROWS, SL), BF16), vm((NT, 1, 128), F32), vm((NZ, ROWS, SL), BF16),
        vm((NT, ROWS, 1024), BF16), vm((NT, ROWS, 1024), BF16), vm((NT, ROWS, SL), BF16),
        vm((NX, SLOTS, SL), BF16), vm((NT, NX, SLOTS, SL), BF16), vm((NT, NX * SLOTS, 128), BF16),
        vm((NX, SLOTS, SL), BF16), vm((NX, SLOTS, SL), BF16), vm((NZ, ROWS, SL), BF16), vm((NZ, ROWS, SL), BF16),
        pltpu.SemaphoreType.DMA((24,)),
        pltpu.SemaphoreType.DMA((26,)), pltpu.SemaphoreType.DMA((26,)),
        pltpu.SemaphoreType.DMA((49,)), pltpu.SemaphoreType.DMA((49,)),
        pltpu.SemaphoreType.DMA((49,)), pltpu.SemaphoreType.DMA((49,)),
    ]
    mixed_out, new_state = pl.pallas_call(
        kernel,
        out_shape=(
            jax.ShapeDtypeStruct((ROWS, SL), BF16),
            jax.ShapeDtypeStruct((ROWS, 2, HEAD, HEAD), F32),
        ),
        in_specs=in_specs,
        out_specs=(pl.BlockSpec(memory_space=pltpu.VMEM), pl.BlockSpec(memory_space=pltpu.VMEM)),
        scratch_shapes=scratch,
        compiler_params=pltpu.CompilerParams(
            collective_id=0, has_side_effects=True, vmem_limit_bytes=48 * 1024 * 1024),
        name="layer",
    )(
        tokens, delta_state, attn_gain.reshape(1, D), query_weight, key_weight, value_weight, decay_weight.T,
        beta_weight.T, decay_rate, head_gain.reshape(1, HEAD), output_weight, ffn_gain.reshape(1, D), info,
        expert_gate.reshape(D, 128), expert_up.reshape(D, 128), expert_down.reshape(128, D), dense_gate, dense_up,
        dense_down, dense_mix.reshape(1, SL),
    )
    return mixed_out, new_state


def solution(mesh):
    return jax.shard_map(
        per_device,
        mesh=mesh,
        in_specs=(
            P("ep", None),
            P("ep", "tp", None, None),
            P(),
            P("ep", "tp"),
            P("ep", "tp"),
            P("ep", "tp"),
            P(),
            P(),
            P("tp"),
            P(),
            P("tp", None),
            P(),
            P("ep", None),
            P("ep"),
            P("ep", None),
            P("ep", None, "tp"),
            P("ep", None, "tp"),
            P("ep", "tp", None),
            P("tp", "ep"),
            P("tp", "ep"),
            P("ep", "tp"),
            P("tp"),
        ),
        out_specs=(P("ep", "tp"), P("ep", "tp", None, None)),
        check_vma=False,
    )
```

time: 271 us -> 105 us (0.39)
  waiting for transfers between devices: 161 us -> 0 us
  Pallas kernels: 0 us -> 80.8 us
  starting transfers between devices: 40.5 us -> 0 us
  blocking collectives: 21.2 us -> 0 us
  matrix products: 19.1 us -> 0 us
  other arithmetic: 10.1 us -> 0.76 us
  local copies, waits for them, and re-layouts: 16.5 us -> 21.2 us
    all_to_all x8 -> x0, waiting for transfers between devices: 161 us -> none  [the longest x3 71.6 us: sent_to_all(): lax.all_to_all(jnp.broadcast_to(shard[None], (count, *shard.shape)), axis...]
    pallas_call x0 -> x1, Pallas kernels: none -> 80.8 us  [per_device(): pl.pallas_call(kernel, out_shape=(jax.ShapeDtypeStruct((ROWS, SL), BF16),...]
    all_to_all x8 -> x0, starting transfers between devices: 40.5 us -> none  [the longest x3 14.7 us: summed_on_arrival(): lax.all_to_all(tiles, axis, split_axis=0, concat_axis=0, tiled=True)]
    all_to_all x1 -> x0, blocking collectives: 21.2 us -> none  [per_device(): lax.all_to_all(normed, 'ep', split_axis=1, concat_axis=0, tiled=True)]
    dot_general x11 -> x0, matrix products: 19.1 us -> none  [the longest x1 3.56 us: per_device(): jnp.einsum('snf,fd->snd', expert_hidden, expert_down[0], preferred_elemen...]
    unnamed x35 -> x37, local copies, waits for them, and re-layouts: 2.16 us -> 20.3 us
    reduce_sum x13 -> x0, other arithmetic: 6.59 us -> none  [the longest x2 4.06 us: over_copies(): return jnp.sum(everything.astype(jnp.float32), axis=0)]
    broadcast_in_dim x4 -> x2, local copies, waits for them, and re-layouts: 6.21 us -> 0.74 us  [the longest x1 0.73 us: per_device(): group_prob[:, None]]
  transfers between devices with their start and end apart: 8 -> 0, of which waited for: 8 -> 0; matrix products, arithmetic and copies ran while one was open for 8% -> 0% of each run, Pallas kernels for 0% -> 0%
where the time goes in v1:
time: 105 us; the launch traced here: 103 us
  Pallas kernels  80.8 us (77%)
  local copies, waits for them, and re-layouts  21.2 us (20%)
    pallas_call x1, Pallas kernels, per_device(): pl.pallas_call(kernel, out_shape=(jax.ShapeDtypeStruct((ROWS, SL), BF16),...  80.8 us
    unnamed x37, local copies, waits for them, and re-layouts  20.3 us

profile of v1, /device:TPU:2, one launch (start us, length us, event | category | flops | bytes accessed | tf_op | source)
XLA Modules:
  0.0 103.5 jit_solution(12967033705634170082)
XLA Ops:
  0.6 0.1 pad.3.clone
  0.7 0.7 convert_element_type.3
  1.4 0.1 copy.24
  1.5 0.7 copy.26
  2.2 0.8 copy.25
  3.0 0.1 maximum_maximum_fusion.info_h
  3.1 0.0 copy-start
  3.1 1.2 %copy-done = bf16[1,4096,128]{2,1,0:T(8,128)(2,1)S(1)} copy-done((bf16[1,4096,128]{2,1,0:T(8,128)(2,1)S(1)}, bf16[1,4096,128]{2,1,0:T(8,128)(2,1)}, u32[]{:S(2)}) %copy-start) | copy-done | bytes 1048600
  4.3 0.0 copy-start.1
  4.3 1.2 %copy-done.1 = bf16[1,4096,128]{2,1,0:T(8,128)(2,1)S(1)} copy-done((bf16[1,4096,128]{2,1,0:T(8,128)(2,1)S(1)}, bf16[1,4096,128]{2,1,0:T(8,128)(2,1)}, u32[]{:S(2)}) %copy-start.1) | copy-done | bytes 1048600
  5.5 0.0 copy-start.2
  5.5 1.2 %copy-done.2 = bf16[1,128,4096]{2,1,0:T(8,128)(2,1)S(1)} copy-done((bf16[1,128,4096]{2,1,0:T(8,128)(2,1)S(1)}, bf16[1,128,4096]{2,1,0:T(8,128)(2,1)}, u32[]{:S(2)}) %copy-start.2) | copy-done | bytes 1048600
  6.7 0.0 copy-start.3
  6.7 0.9 copy-done.3
  7.7 0.0 copy-start.4
  7.7 0.9 copy-done.4
  8.6 0.0 copy-start.5
  8.6 0.9 copy-done.5
  9.5 0.0 copy-start.6
  9.5 0.9 copy-done.6
  10.4 0.0 copy-start.7
  10.4 0.9 copy-done.7
  11.3 0.0 copy-start.8
  11.3 0.9 copy-done.8
  12.2 0.0 copy-start.9
  12.2 0.8 copy-done.9
  13.0 0.0 copy-start.10
  13.0 0.8 copy-done.10
  13.9 0.0 copy-start.11
  13.9 0.8 copy-done.11
  14.7 0.0 copy-start.12
  14.7 0.7 copy-done.12
  15.4 0.0 copy-start.13
  15.4 0.7 copy-done.13
  16.1 0.0 copy-start.14
  16.1 0.7 copy-done.14
  16.8 0.0 copy-start.15
  16.8 0.7 copy-done.15
  17.5 0.0 copy-start.16
  17.5 0.7 copy-done.16
  18.1 80.8 %layer.1 = (bf16[24,512]{1,0:T(8,128)(2,1)S(1)}, f32[24,2,128,128]{3,2,1,0:T(8,128)}) custom-call(bf16[24,4096]{1,0:T(8,128)(2,1)S(1)} %copy-done.3, f32[24,2,128,128]{3,2,1,0:T(8,128)} %state_h.1, f32[1,4096]{1,0:T(1,128)S(1)} %bitcast.15, bf16[128,256]{1,0:T(8,128)(2,1)S(1)} %copy-done.9, bf16[128,256]{1,0:T(8,128)(2,1)S(1)} %copy-done.10, ...), custom_call_target="tpu_custom_call" | custom-call | tf_op jit(solution)/shard_map/layer/pallas_call | solution.py:464
  98.9 0.6 copy.29
  99.5 3.9 %copy.30 = f32[24,2,128,128]{3,2,1,0:T(8,128)} copy(f32[24,2,128,128]{3,2,1,0:T(8,128)} %get-tuple-element.5) | data formatting | bytes 6291456
  (1 shorter events, 0.0 us)
Async XLA Ops:
  3.1 1.2 %copy-start = (bf16[1,4096,128]{2,1,0:T(8,128)(2,1)S(1)}, bf16[1,4096,128]{2,1,0:T(8,128)(2,1)}, u32[]{:S(2)}) copy-start(bf16[1,4096,128]{2,1,0:T(8,128)(2,1)} %param.37) | copy-start | bytes 3145732
  4.3 1.2 %copy-start.1 = (bf16[1,4096,128]{2,1,0:T(8,128)(2,1)S(1)}, bf16[1,4096,128]{2,1,0:T(8,128)(2,1)}, u32[]{:S(2)}) copy-start(bf16[1,4096,128]{2,1,0:T(8,128)(2,1)} %param.38) | copy-start | bytes 3145732
  5.5 1.2 %copy-start.2 = (bf16[1,128,4096]{2,1,0:T(8,128)(2,1)S(1)}, bf16[1,128,4096]{2,1,0:T(8,128)(2,1)}, u32[]{:S(2)}) copy-start(bf16[1,128,4096]{2,1,0:T(8,128)(2,1)} %param.39) | copy-start | bytes 3145732
  6.7 0.9 copy-start.3
  7.7 0.9 copy-start.4
  8.6 0.9 copy-start.5
  9.5 0.9 copy-start.6
  10.4 0.9 copy-start.7
  11.3 0.9 copy-start.8
  12.2 0.8 copy-start.9
  13.0 0.8 copy-start.10
  13.9 0.8 copy-start.11
  14.7 0.7 copy-start.12
  15.4 0.7 copy-start.13
  16.1 0.7 copy-start.14
  16.8 0.7 copy-start.15
  17.5 0.7 copy-start.16

commit v2 on v1

v2 whole, which is shorter than its diff:
```python
import jax
import jax.numpy as jnp
from jax import lax
from jax.experimental import pallas as pl
from jax.experimental.pallas import tpu as pltpu
from jax.sharding import PartitionSpec as P

EPS = 1e-06
MESH = pl.DeviceIdType.MESH
F32 = jnp.float32
BF16 = jnp.bfloat16

NX, NZ, NY, NT = 4, 8, 4, 8
ROWS = 24
D = 4096
SL = 512
HEAD = 128
CAP = 3
SLOTS = NZ * CAP
N_SEND, N_RECV = 23, 52
X_ORDER = (2, 1, 3)
Z_ORDER = (4, 3, 5, 2, 6, 1, 7)
Y_ORDER = (2, 1, 3)
E_ORDER = tuple(
    (dx, dy) for far in (4, 3, 2, 1) for dx in range(NX) for dy in range(NY)
    if min(dx, NX - dx) + min(dy, NY - dy) == far)
T_ORDER = ((2, 0), (2, 1), (1, 0), (1, 1), (3, 0), (3, 1), (0, 1))


def kernel(
    tok_h, state_h, again_h, wq_h, wk_h, wv_h, dT_h, bT_h, rate_h, hgain_h, wo_h, fgain_h, ids_h,
    lgt_h, prob_h,
    eg_h, eu_h, ed_h, dg_h, du_h, dd_h, mix_h,
    out_ref, state_o,
    tok, tokf, again, wqkv, db, rate, hgain, wo, fgain, idv, lgv, prv, wgu, wdn, mixv, egu, edn, state,
    spread, act, psrc, pdst, rout, asrc, adst, ssb, rsb, xall, dsrc, dmate, dpair, ddst, qsrc, qdst, hall, esrc, eall, ehall, rsrc, rdst, fsrc, fdst,
    lsem, ssem, rsem,
):
    ep = lax.axis_index("ep")
    tp = lax.axis_index("tp")
    z = ep // NX
    x = lax.rem(ep, NX)

    def at_x(d):
        return {"ep": z * NX + lax.rem(x + d, NX), "tp": tp}

    def at_z(d):
        return {"ep": lax.rem(z + d, NZ) * NX + x, "tp": tp}

    y = tp // 2
    core = lax.rem(tp, 2)

    def t_index(d):
        return lax.rem(y + d[0], NY) * 2 + lax.rem(core + d[1], 2)

    def at_t(d):
        return {"ep": ep, "tp": t_index(d)}

    other = 1 - core
    mate = {"ep": ep, "tp": y * 2 + other}

    def y_index(d):
        return lax.rem(y + d, NY) * 2 + core

    def at_y(d):
        return {"ep": ep, "tp": y_index(d)}

    def remote(src, dst, ss, rs, dev):
        return pltpu.make_async_remote_copy(
            src_ref=src, dst_ref=dst, send_sem=ss, recv_sem=rs, device_id=dev, device_id_type=MESH
        )

    count = {"send": 0, "recv": 0}
    last = []

    def new(kind):
        count[kind] += 1
        return count[kind] - 1

    def send(src, dst, si, ri, dev):
        copy = remote(src, dst, ssem.at[si], rsem.at[ri], dev)
        copy.start()
        return copy

    def leaves(whole, si):
        last.append(remote(whole, whole, ssem.at[si], rsem.at[0], mate))

    def exchange(order, at, src, dst, whole):
        si, ri = new("send"), new("recv")
        for d in order:
            send(src(d), dst, si, ri, at(d))
        leaves(whole, si)
        return remote(whole, whole, ssem.at[si], rsem.at[ri], mate)

    local = []

    def load(src, dst):
        c = pltpu.make_async_copy(src, dst, lsem.at[len(local)])
        c.start()
        local.append(c)
        return c

    bar = pltpu.get_barrier_semaphore()
    for d in X_ORDER:
        pl.semaphore_signal(bar, inc=1, device_id=at_x(d), device_id_type=MESH)
    for d in Z_ORDER:
        pl.semaphore_signal(bar, inc=1, device_id=at_z(d), device_id_type=MESH)
    for d in T_ORDER:
        pl.semaphore_signal(bar, inc=1, device_id=at_t(d), device_id_type=MESH)

    l_tok = load(tok_h, tok)
    l_again = load(again_h, again)
    l_w = [load(w, wqkv.at[m, x]) for m, w in enumerate((wk_h, wq_h, wv_h))]

    pl.semaphore_wait(bar, NX + NZ + NT - 3)

    left = lax.rem(x + NX - 1, NX)
    right = lax.rem(x + 1, NX)

    def gather_start(buf, si):
        return (
            send(buf.at[x], buf.at[x], si, new("recv"), at_x(1)),
            send(buf.at[x], buf.at[x], si, new("recv"), at_x(NX - 1)),
        )

    def gather_relay(buf, si, c0, c1):
        h = buf.shape[1] // 2
        low, high = buf.at[left, pl.ds(0, h)], buf.at[right, pl.ds(h, h)]
        c0.wait_recv()
        r0 = send(low, low, si, new("recv"), at_x(1))
        c1.wait_recv()
        r1 = send(high, high, si, new("recv"), at_x(NX - 1))
        return r0, r1

    for c in l_w:
        c.wait()
    s_w = new("send")
    leaves(wqkv.at[:, pl.ds(0, 3)], s_w)
    g_w = [gather_start(wqkv.at[m], s_w) for m in range(2)]

    l_tok.wait()
    l_again.wait()
    t32 = tok[...].astype(F32)
    ms = jnp.sum(t32 * t32, axis=1, keepdims=True) * (1.0 / D)
    normed = (t32 * lax.rsqrt(ms + EPS) * again[...]).astype(BF16)
    for b in range(NZ):
        for h in range(2):
            spread[h, b] = normed[:, b * SL + h * 256 : b * SL + (h + 1) * 256]

    c_spread = exchange(
        Z_ORDER, at_z, lambda d: spread.at[core, lax.rem(z + d, NZ)], act.at[core, z], act.at[core, pl.ds(0, NZ - 1)])
    act[core, z] = spread[core, z]

    c_ed = exchange(
        T_ORDER, at_t, lambda d: ed_h.at[:, pl.ds(pl.multiple_of(t_index(d) * SL, SL), SL)], edn.at[tp],
        edn.at[pl.ds(0, NT - 1)])

    l_db = [load(dT_h, db.at[0]), load(bT_h, db.at[1]), load(rate_h, rate)]
    l_info = [load(ids_h, idv), load(lgt_h, lgv), load(prob_h, prv)]
    l_gu = [load(dg_h, wgu.at[x, :, pl.ds(0, 128)]), load(du_h, wgu.at[x, :, pl.ds(128, 128)])]
    l_dn = load(dd_h, wdn.at[x])
    l_state = load(state_h, state)
    l_wo = load(wo_h, wo)
    l_small = [
        load(hgain_h, hgain),
        load(fgain_h.at[:, pl.ds(pl.multiple_of(tp * SL, SL), SL)], fgain),
        load(mix_h, mixv),
        load(tok_h.at[:, pl.ds(pl.multiple_of(tp * SL, SL), SL)], tokf),
    ]
    l_ed = load(ed_h.at[:, pl.ds(pl.multiple_of(tp * SL, SL), SL)], edn.at[tp])
    l_egu = [load(eg_h, egu.at[:, pl.ds(0, 128)]), load(eu_h, egu.at[:, pl.ds(128, 128)])]

    for c in l_db:
        c.wait()
    dims = (((1,), (1,)), ((), ()))
    dpre = lax.dot_general(normed, db[0], dims, preferred_element_type=F32)
    bpre = lax.dot_general(normed, db[1], dims, preferred_element_type=F32)
    lane16 = lax.broadcasted_iota(jnp.int32, dpre.shape, 1)
    decay, beta = [], []
    for h in range(2):
        pick = lane16 == tp * 2 + h
        dp = jnp.sum(jnp.where(pick, dpre, 0.0), axis=1, keepdims=True)
        bp = jnp.sum(jnp.where(pick, bpre, 0.0), axis=1, keepdims=True)
        soft = jnp.maximum(dp, 0.0) + jnp.log(1.0 + jnp.exp(-jnp.abs(dp)))
        decay.append(jnp.exp(-rate[:, h : h + 1] * soft))
        beta.append(1.0 / (1.0 + jnp.exp(-bp)))

    for c in l_info:
        c.wait()
    ex = jnp.exp(lgv[...])
    wrow = prv[...] * ex / (ex[0:1] + ex[1:2])
    idf = idv[...].astype(F32)
    square = (ROWS, ROWS)
    eye24 = lax.broadcasted_iota(jnp.int32, square, 0) == lax.broadcasted_iota(jnp.int32, square, 1)

    def column(row):
        return jnp.sum(jnp.where(eye24, jnp.broadcast_to(row, square), 0.0), axis=1, keepdims=True)

    id0, id1 = column(idf[0:1]), column(idf[1:2])
    w0, w1 = column(wrow[0:1]), column(wrow[1:2])
    lanef = lax.broadcasted_iota(jnp.int32, (ROWS, 128), 1).astype(F32)
    rowi = lax.broadcasted_iota(jnp.int32, (ROWS, 128), 0)
    oh = jnp.where((lanef == id0) | (lanef == id1), 1.0, 0.0)
    rank = jnp.zeros((ROWS, 128), F32)
    for i in range(ROWS - 1):
        rank = rank + jnp.where(rowi > i, oh[i : i + 1, :], 0.0)
    table = (rank + 1.0) * oh
    for idk, wk in ((id0, w0), (id1, w1)):
        whi = wk.astype(BF16).astype(F32)
        table = table + jnp.where(lanef == idk + 32.0, whi, 0.0)
        table = table + jnp.where(lanef == idk + 64.0, wk - whi, 0.0)
    rout[z] = table.astype(BF16)

    r_w = [gather_relay(wqkv.at[0], s_w, *g_w[0])]
    g_v = gather_start(wqkv.at[2], s_w)
    r_w.append(gather_relay(wqkv.at[1], s_w, *g_w[1]))
    c_spread.wait_recv()
    i = new("send")
    c_share = send(act.at[core], act.at[core], i, new("recv"), mate)
    leaves(act.at[core], i)
    for c in r_w[0]:
        c.wait_recv()
    ntok = NZ * ROWS

    def half(m, h):
        return jnp.dot(
            act[h].reshape(ntok, 256), wqkv[m, pl.ds(h * 2, 2)].reshape(256, 256), preferred_element_type=F32)

    c_p = []
    for m in range(3):
        if m:
            for c in r_w[m]:
                c.wait_recv()
        part = half(m, core)
        if m == 0:
            c_share.wait_recv()
        part = part + half(m, other)
        psrc[m] = part.astype(BF16).reshape(NZ, ROWS, 2 * HEAD)
        c_p.append(exchange(
            Z_ORDER, at_z, lambda d: psrc.at[m, lax.rem(z + d, NZ)], pdst.at[m, z], pdst.at[m, pl.ds(0, NZ - 1)]))
        pdst[m, z] = psrc[m, z]
        if m == 0:
            r_w.append(gather_relay(wqkv.at[2], s_w, *g_v))
    for c in l_gu:
        c.wait()
    l_dn.wait()
    s_gu, s_dn = new("send"), new("send")
    g_gu = gather_start(wgu, s_gu)
    g_dn = gather_start(wdn, s_dn)
    leaves(wgu.at[pl.ds(0, 3)], s_gu)
    leaves(wdn.at[pl.ds(0, 3)], s_dn)

    c_r = exchange(Z_ORDER, at_z, lambda d: rout.at[z], rout.at[z], rout.at[pl.ds(0, NZ - 1)])

    def arrived(m):
        c_p[m].wait_recv()
        total = pdst[m, 0].astype(F32)
        for b in range(1, NZ):
            total = total + pdst[m, b].astype(F32)
        return total.astype(BF16).astype(F32)

    def unit(rows):
        return rows * lax.rsqrt(jnp.sum(rows * rows, axis=1, keepdims=True) + EPS)

    def read_state(h, cols):
        return jnp.concatenate(
            [jnp.sum(state[b, h] * cols[:, b : b + 1], axis=0, keepdims=True) for b in range(ROWS)], axis=0)

    l_state.wait()
    rows_k = arrived(0)
    ku = [unit(rows_k[:, h * HEAD : (h + 1) * HEAD]) for h in range(2)]
    kT = [u.T for u in ku]
    rec = [read_state(h, kT[h]) for h in range(2)]
    rows_q = arrived(1)
    qu = [unit(rows_q[:, h * HEAD : (h + 1) * HEAD]) * HEAD ** (-0.5) for h in range(2)]
    red = [read_state(h, qu[h].T) for h in range(2)]
    for c in l_small:
        c.wait()
    l_wo.wait()
    rows_v = arrived(2)
    heads, corrs = [], []
    for h in range(2):
        kq = jnp.sum(ku[h] * qu[h], axis=1, keepdims=True)
        corr = beta[h] * (rows_v[:, h * HEAD : (h + 1) * HEAD] - decay[h] * rec[h])
        ro = decay[h] * red[h] + kq * corr
        ro = ro * lax.rsqrt(jnp.mean(ro * ro, axis=1, keepdims=True) + EPS) * hgain[...]
        heads.append(ro.astype(BF16))
        corrs.append(corr)

    hcat = jnp.concatenate(heads, axis=1)
    si, ri = new("send"), new("recv")
    for d in T_ORDER + ((0, 0),):
        td = t_index(d)
        cols = wo[:, pl.ds(pl.multiple_of(td * SL, SL), SL)]
        asrc[td] = jnp.dot(hcat, cols, preferred_element_type=F32).astype(BF16)
        if d != (0, 0):
            send(asrc.at[td], adst.at[tp], si, ri, at_t(d))
    whole = adst.at[pl.ds(0, NT - 1)]
    leaves(whole, si)
    c_a = remote(whole, whole, ssem.at[si], rsem.at[ri], mate)
    adst[tp] = asrc[tp]

    for h in range(2):
        for b in range(ROWS):
            state[b, h] = state[b, h] * decay[h][b : b + 1, :] + kT[h][:, b : b + 1] * corrs[h][b : b + 1, :]
    w_state = pltpu.make_async_copy(state, state_o, lsem.at[len(local)])
    w_state.start()

    c_a.wait_recv()
    asum = adst[0].astype(F32)
    for b in range(1, NT):
        asum = asum + adst[b].astype(F32)
    middle = tokf[...].astype(F32) + asum
    ss = jnp.sum(middle * middle, axis=1, keepdims=True)
    eye = lax.broadcasted_iota(jnp.int32, (ROWS, 128), 0) == lax.broadcasted_iota(jnp.int32, (ROWS, 128), 1)
    ssb[tp] = jnp.sum(jnp.where(eye, ss, 0.0), axis=0, keepdims=True)
    c_s = exchange(T_ORDER, at_t, lambda d: ssb.at[tp], ssb.at[tp], ssb.at[pl.ds(0, NT - 1)])
    xall[z] = (middle * fgain[...]).astype(BF16)
    c_x = exchange(Z_ORDER, at_z, lambda d: xall.at[z], xall.at[z], xall.at[pl.ds(0, NZ - 1)])
    r_gu = gather_relay(wgu, s_gu, *g_gu)
    r_dn = gather_relay(wdn, s_dn, *g_dn)
    c_s.wait_recv()
    srow = ssb[0]
    for b in range(1, NT):
        srow = srow + ssb[b]
    rsb[z] = lax.rsqrt(srow * (1.0 / D) + EPS)
    c_q = exchange(Z_ORDER, at_z, lambda d: rsb.at[z], rsb.at[z], rsb.at[pl.ds(0, NZ - 1)])

    c_r.wait_recv()
    rt = rout[...].astype(F32)
    shape3 = (NZ, ROWS, 128)
    lane3 = lax.broadcasted_iota(jnp.int32, shape3, 2)
    blk3 = lax.broadcasted_iota(jnp.int32, shape3, 0)
    sel = jnp.zeros(shape3, F32)
    hi = jnp.zeros(shape3, F32)
    lo = jnp.zeros(shape3, F32)
    for xx in range(NX):
        e = z * NX + xx
        r = jnp.sum(jnp.where(lane3 == e, rt, 0.0), axis=2, keepdims=True)
        wh = jnp.sum(jnp.where(lane3 == e + 32, rt, 0.0), axis=2, keepdims=True)
        wl = jnp.sum(jnp.where(lane3 == e + 64, rt, 0.0), axis=2, keepdims=True)
        place = blk3.astype(F32) * CAP + (r - 1.0) + float(xx * SLOTS)
        hit = (lane3.astype(F32) == place) & (r > 0.5)
        sel = sel + jnp.where(hit, 1.0, 0.0)
        hi = hi + jnp.where(hit, wh, 0.0)
        lo = lo + jnp.where(hit, wl, 0.0)
    selT = sel.reshape(ntok, 128).T.astype(BF16)
    hi2 = hi.reshape(ntok, 128).astype(BF16)
    lo2 = lo.reshape(ntok, 128).astype(BF16)

    c_x.wait_recv()
    xs2 = xall[...].reshape(ntok, SL)
    picked = jnp.dot(selT, xs2, preferred_element_type=F32).astype(BF16)
    for xx in range(NX):
        esrc[xx] = picked[xx * SLOTS : (xx + 1) * SLOTS]
    si = new("send")
    r_e = {d: new("recv") for d in (0,) + Y_ORDER}
    for dx, dy in E_ORDER:
        xd = lax.rem(x + dx, NX)
        dev = {"ep": z * NX + xd, "tp": y_index(dy)}
        send(esrc.at[xd], eall.at[tp, x], si, r_e[dy], dev)
    leaves(eall.at[pl.ds(0, 3)], si)
    leaves_e = eall.at[0, pl.ds(0, NX - 1)]
    leaves(leaves_e, si)
    eall[tp, x] = esrc[x]

    for c in r_gu:
        c.wait_recv()
    for xx in range(NX):
        part = jnp.dot(xs2, wgu[xx], preferred_element_type=F32).astype(BF16).reshape(NZ, ROWS, 256)
        for b in range(NZ):
            dsrc[b % 2, b // 2, :, xx * 256 : (xx + 1) * 256] = part[b]
    c_q.wait_recv()
    eye3 = lax.broadcasted_iota(jnp.int32, shape3, 1) == lane3
    rcol = jnp.sum(jnp.where(eye3, jnp.broadcast_to(rsb[...], shape3), 0.0), axis=2, keepdims=True)
    rhi = rcol.astype(BF16).astype(F32)
    pair = jnp.where(lane3 < 64, rhi, rcol - rhi).astype(BF16).reshape(ntok, 128)
    rslot = jnp.dot(selT, pair, preferred_element_type=F32)
    rslot = jnp.broadcast_to(rslot[:, 0:1] + rslot[:, 127:128], (128, 128))
    for xx in range(NX):
        qsrc[xx] = rslot[xx * SLOTS : (xx + 1) * SLOTS]
    c_sc = exchange(
        X_ORDER, at_x, lambda d: qsrc.at[lax.rem(x + d, NX)], qdst.at[x], qdst.at[pl.ds(0, NX - 1)])
    qdst[x] = qsrc[x]
    i = new("send")
    c_dm = send(dsrc.at[other], dmate, i, new("recv"), mate)
    leaves(dmate, i)
    for c in l_egu:
        c.wait()
    c_dm.wait_recv()
    for b in range(NY):
        dpair[b] = (dsrc[core, b].astype(F32) + dmate[b].astype(F32)).astype(BF16)
    c_d = exchange(
        Y_ORDER, at_y, lambda d: dpair.at[lax.rem(y + d, NY)], ddst.at[y], ddst.at[pl.ds(0, NY - 1)])
    ddst[y] = dpair[y]

    def hidden_part(t):
        rows = egu[pl.ds(pl.multiple_of(t * SL, SL), SL), :]
        return jnp.dot(eall[t].reshape(NX * SLOTS, SL), rows, preferred_element_type=F32)

    s_m = new("send")
    acc = jnp.zeros((NX * SLOTS, 256), F32)
    c_m = []
    for dy in (0, 1, 3, 2):
        t = y_index(NY - dy)
        got = eall.at[t] if dy else leaves_e
        remote(got, got, ssem.at[si], rsem.at[r_e[dy]], mate).wait_recv()
        c_m.append(send(eall.at[t], eall.at[t], s_m, new("recv"), mate))
        acc = acc + hidden_part(t)
    leaves(eall.at[pl.ds(0, NY)], s_m)
    for c, dy in zip(c_m, (0, 1, 3, 2)):
        c.wait_recv()
        acc = acc + hidden_part(lax.rem(y + NY - dy, NY) * 2 + other)

    def tp_gather(buf):
        si, rm = new("send"), new("recv")
        out = [send(buf.at[tp], buf.at[tp], si, new("recv"), at_y(d)) for d in Y_ORDER]
        send(buf.at[tp], buf.at[tp], si, rm, mate)
        return si, rm, out

    def tp_gathered(buf, si, rm, out):
        for c, d in zip(out, Y_ORDER):
            c.wait_recv()
            t = y_index(NY - d)
            send(buf.at[t], buf.at[t], si, rm, mate)
        leaves(buf.at[pl.ds(0, NT - 1)], si)
        got = buf.at[pl.ds(0, NY)]
        remote(got, got, ssem.at[si], rsem.at[rm], mate).wait_recv()

    c_sc.wait_recv()
    scale = qdst[...].reshape(NX * SLOTS, 128)
    ga, ua = acc[:, :128] * scale, acc[:, 128:] * scale
    ehall[tp] = (ga / (1.0 + jnp.exp(-ga)) * ua).astype(BF16)
    c_eh = tp_gather(ehall)

    c_d.wait_recv()
    dsum = ddst[0].astype(F32)
    for b in range(1, NY):
        dsum = dsum + ddst[b].astype(F32)
    dsum = dsum * jnp.sum(jnp.where(eye, jnp.broadcast_to(rsb[tp], (ROWS, 128)), 0.0), axis=1, keepdims=True)
    hid = []
    for xx in range(NX):
        g = dsum[:, xx * 256 : xx * 256 + 128]
        u = dsum[:, xx * 256 + 128 : xx * 256 + 256]
        hid.append((g / (1.0 + jnp.exp(-g)) * u).astype(BF16))
    hall[tp] = jnp.concatenate(hid, axis=1)
    c_h = tp_gather(hall)

    l_ed.wait()
    c_ed.wait_recv()
    tp_gathered(ehall, *c_eh)
    eres = jnp.zeros((NX * SLOTS, SL), F32)
    for t in range(NT):
        eres = eres + jnp.dot(ehall[t], edn[t], preferred_element_type=F32)
    rsrc[...] = eres.astype(BF16).reshape(NX, SLOTS, SL)
    c_b = exchange(
        X_ORDER, at_x, lambda d: rsrc.at[lax.rem(x + d, NX)], rdst.at[x], rdst.at[pl.ds(0, NX - 1)])
    rdst[x] = rsrc[x]

    for c in r_dn:
        c.wait_recv()
    tp_gathered(hall, *c_h)
    down = jnp.dot(
        hall[...].reshape(ntok, SL), wdn[...].reshape(SL, SL), preferred_element_type=F32)
    down = down * (1.0 / (1.0 + jnp.exp(-mixv[...])))
    c_b.wait_recv()
    back = rdst[...].reshape(NX * SLOTS, SL)
    down = down + jnp.dot(hi2[:, : NX * SLOTS], back, preferred_element_type=F32)
    down = down + jnp.dot(lo2[:, : NX * SLOTS], back, preferred_element_type=F32)
    fsrc[...] = down.astype(BF16).reshape(NZ, ROWS, SL)
    c_f = exchange(
        Z_ORDER, at_z, lambda d: fsrc.at[lax.rem(z + d, NZ)], fdst.at[z], fdst.at[pl.ds(0, NZ - 1)])
    fdst[z] = fsrc[z]
    c_f.wait_recv()
    total = middle
    for b in range(NZ):
        total = total + fdst[b].astype(F32)
    out_ref[...] = total.astype(BF16)

    for c in last:
        c.wait_send()
    w_state.wait()
    assert count == {"send": N_SEND, "recv": N_RECV}, count


def per_device(
    tokens, delta_state, attn_gain, query_weight, key_weight, value_weight, decay_weight, beta_weight, decay_rate,
    head_gain, output_weight, ffn_gain, expert_ids, group_prob, expert_logit, expert_gate, expert_up, expert_down,
    dense_gate, dense_up, dense_down, dense_mix,
):
    hbm = pl.BlockSpec(memory_space=pltpu.HBM)
    in_specs = [hbm] * 22
    vm = pltpu.VMEM
    scratch = [
        vm((ROWS, D), BF16), vm((ROWS, SL), BF16), vm((1, D), F32), vm((3, NX, 128, 256), BF16), vm((2, 16, D), BF16),
        vm((1, 2), F32),        vm((1, HEAD), F32), vm((256, D), BF16), vm((1, SL), F32), vm((2, ROWS), jnp.int32),
        vm((2, ROWS), F32), vm((1, ROWS), F32), vm((NX, SL, 256), BF16), vm((NX, 128, SL), BF16), vm((1, SL), F32), vm((D, 256), BF16), vm((NT, 128, SL), BF16),
        vm((ROWS, 2, HEAD, HEAD), F32),
        vm((2, NZ, ROWS, 256), BF16), vm((2, NZ, ROWS, 256), BF16),
        vm((3, NZ, ROWS, 256), BF16), vm((3, NZ, ROWS, 256), BF16), vm((NZ, ROWS, 128), BF16),
        vm((NT, ROWS, SL), BF16), vm((NT, ROWS, SL), BF16), vm((NT, 1, 128), F32), vm((NZ, 1, 128), F32),
        vm((NZ, ROWS, SL), BF16),
        vm((2, NY, ROWS, 1024), BF16), vm((NY, ROWS, 1024), BF16), vm((NY, ROWS, 1024), BF16),
        vm((NY, ROWS, 1024), BF16), vm((NX, SLOTS, 128), F32), vm((NX, SLOTS, 128), F32), vm((NT, ROWS, SL), BF16),
        vm((NX, SLOTS, SL), BF16), vm((NT, NX, SLOTS, SL), BF16), vm((NT, NX * SLOTS, 128), BF16),
        vm((NX, SLOTS, SL), BF16), vm((NX, SLOTS, SL), BF16), vm((NZ, ROWS, SL), BF16), vm((NZ, ROWS, SL), BF16),
        pltpu.SemaphoreType.DMA((32,)),
        pltpu.SemaphoreType.DMA((N_SEND,)), pltpu.SemaphoreType.DMA((N_RECV,)),
    ]
    operands = (
        tokens, delta_state, attn_gain.reshape(1, D), query_weight, key_weight, value_weight, decay_weight.T,
        beta_weight.T, decay_rate.reshape(1, 2), head_gain.reshape(1, HEAD), output_weight, ffn_gain.reshape(1, D), expert_ids.T,
        expert_logit.T, group_prob.reshape(1, ROWS), expert_gate.reshape(D, 128), expert_up.reshape(D, 128),
        expert_down.reshape(128, D), dense_gate, dense_up, dense_down, dense_mix.reshape(1, SL),
    )
    operands = [pltpu.with_memory_space_constraint(o, pltpu.HBM) for o in operands]
    mixed_out, new_state = pl.pallas_call(
        kernel,
        out_shape=(
            jax.ShapeDtypeStruct((ROWS, SL), BF16),
            jax.ShapeDtypeStruct((ROWS, 2, HEAD, HEAD), F32),
        ),
        in_specs=in_specs,
        out_specs=(pl.BlockSpec(memory_space=pltpu.VMEM), pl.BlockSpec(memory_space=pl.ANY)),
        scratch_shapes=scratch,
        compiler_params=pltpu.CompilerParams(
            collective_id=0, has_side_effects=True, vmem_limit_bytes=24 * 1024 * 1024),
        name="layer",
    )(*operands)
    return mixed_out, new_state


def solution(mesh):
    return jax.shard_map(
        per_device,
        mesh=mesh,
        in_specs=(
            P("ep", None),
            P("ep", "tp", None, None),
            P(),
            P("ep", "tp"),
            P("ep", "tp"),
            P("ep", "tp"),
            P(),
            P(),
            P("tp"),
            P(),
            P("tp", None),
            P(),
            P("ep", None),
            P("ep"),
            P("ep", None),
            P("ep", None, "tp"),
            P("ep", None, "tp"),
            P("ep", "tp", None),
            P("tp", "ep"),
            P("tp", "ep"),
            P("ep", "tp"),
            P("tp"),
        ),
        out_specs=(P("ep", "tp"), P("ep", "tp", None, None)),
        check_vma=False,
    )
```

time: 105 us -> 65.2 us (0.62)
  Pallas kernels: 80.8 us -> 61.5 us
  local copies, waits for them, and re-layouts: 21.2 us -> 2.27 us
    pallas_call x1, Pallas kernels: 80.8 us -> 61.5 us  [per_device(): pl.pallas_call(kernel, out_shape=(jax.ShapeDtypeStruct((ROWS, SL), BF16),...]
    unnamed x37 -> x2, local copies, waits for them, and re-layouts: 20.3 us -> 2.27 us
where the time goes in v2:
time: 65.2 us; the launch traced here: 64.4 us
  Pallas kernels  61.5 us (94%)
  local copies, waits for them, and re-layouts  2.27 us (3%)
    pallas_call x1, Pallas kernels, per_device(): pl.pallas_call(kernel, out_shape=(jax.ShapeDtypeStruct((ROWS, SL), BF16),...  61.5 us
    unnamed x2, local copies, waits for them, and re-layouts  2.27 us

profile of v2, /device:TPU:2, one launch (start us, length us, event | category | flops | bytes accessed | tf_op | source)
XLA Modules:
  0.0 64.4 jit_solution(4876624258562161245)
XLA Ops:
  0.6 61.5 %layer.1 = (bf16[24,512]{1,0:T(8,128)(2,1)S(1)}, f32[24,2,128,128]{3,2,1,0:T(8,128)S(1)}) custom-call(bf16[24,4096]{1,0:T(8,128)(2,1)} %tok_h.1, f32[24,2,128,128]{3,2,1,0:T(8,128)} %state_h.1, f32[1,4096]{1,0:T(1,128)} %bitcast.18, bf16[128,256]{1,0:T(8,128)(2,1)} %wq_h.1, bf16[128,256]{1,0:T(8,128)(2,1)} %wk_h.1, bf16[128,256]{1,0:T(8,128)(2,1)} %wv_h.1, ...), custom_call_target="tpu_custom_call" | custom-call | tf_op jit(solution)/shard_map/layer/pallas_call | solution.py:517
  62.1 0.6 copy.26
  62.7 1.7 %copy.27 = f32[24,2,128,128]{3,2,1,0:T(8,128)} copy(f32[24,2,128,128]{3,2,1,0:T(8,128)S(1)} %get-tuple-element.5) | data formatting | bytes 6291456

commit v3 on v2

--- a/solution.py
+++ b/solution.py
@@ -17,12 +17,12 @@
 HEAD = 128
 CAP = 3
 SLOTS = NZ * CAP
-N_SEND, N_RECV = 23, 52
+N_SEND, N_RECV = 24, 49
 X_ORDER = (2, 1, 3)
 Z_ORDER = (4, 3, 5, 2, 6, 1, 7)
 Y_ORDER = (2, 1, 3)
 E_ORDER = tuple(
-    (dx, dy) for far in (4, 3, 2, 1) for dx in range(NX) for dy in range(NY)
+    (dx, dy) for far in (4, 3, 2, 1) for dy in Y_ORDER + (0,) for dx in X_ORDER + (0,)
     if min(dx, NX - dx) + min(dy, NY - dy) == far)
 T_ORDER = ((2, 0), (2, 1), (1, 0), (1, 1), (3, 0), (3, 1), (0, 1))
 
@@ -135,7 +135,7 @@
     for c in l_w:
         c.wait()
     s_w = new("send")
-    leaves(wqkv.at[:, pl.ds(0, 3)], s_w)
+    leaves(wqkv.at[pl.ds(0, 2), pl.ds(0, 3)], s_w)
     g_w = [gather_start(wqkv.at[m], s_w) for m in range(2)]
 
     l_tok.wait()
@@ -212,7 +212,7 @@
     rout[z] = table.astype(BF16)
 
     r_w = [gather_relay(wqkv.at[0], s_w, *g_w[0])]
-    g_v = gather_start(wqkv.at[2], s_w)
+    c_v = exchange(X_ORDER, at_x, lambda d: wqkv.at[2, x], wqkv.at[2, x], wqkv.at[2, pl.ds(0, 3)])
     r_w.append(gather_relay(wqkv.at[1], s_w, *g_w[1]))
     c_spread.wait_recv()
     i = new("send")
@@ -240,7 +240,7 @@
             Z_ORDER, at_z, lambda d: psrc.at[m, lax.rem(z + d, NZ)], pdst.at[m, z], pdst.at[m, pl.ds(0, NZ - 1)]))
         pdst[m, z] = psrc[m, z]
         if m == 0:
-            r_w.append(gather_relay(wqkv.at[2], s_w, *g_v))
+            r_w.append([c_v])
     for c in l_gu:
         c.wait()
     l_dn.wait()
@@ -418,14 +418,14 @@
         send(buf.at[tp], buf.at[tp], si, rm, mate)
         return si, rm, out
 
-    def tp_gathered(buf, si, rm, out):
+    def tp_hand_on(buf, si, rm, out):
         for c, d in zip(out, Y_ORDER):
             c.wait_recv()
             t = y_index(NY - d)
             send(buf.at[t], buf.at[t], si, rm, mate)
         leaves(buf.at[pl.ds(0, NT - 1)], si)
         got = buf.at[pl.ds(0, NY)]
-        remote(got, got, ssem.at[si], rsem.at[rm], mate).wait_recv()
+        return remote(got, got, ssem.at[si], rsem.at[rm], mate)
 
     c_sc.wait_recv()
     scale = qdst[...].reshape(NX * SLOTS, 128)
@@ -448,7 +448,9 @@
 
     l_ed.wait()
     c_ed.wait_recv()
-    tp_gathered(ehall, *c_eh)
+    c_eh = tp_hand_on(ehall, *c_eh)
+    c_h = tp_hand_on(hall, *c_h)
+    c_eh.wait_recv()
     eres = jnp.zeros((NX * SLOTS, SL), F32)
     for t in range(NT):
         eres = eres + jnp.dot(ehall[t], edn[t], preferred_element_type=F32)
@@ -459,7 +461,7 @@
 
     for c in r_dn:
         c.wait_recv()
-    tp_gathered(hall, *c_h)
+    c_h.wait_recv()
     down = jnp.dot(
         hall[...].reshape(ntok, SL), wdn[...].reshape(SL, SL), preferred_element_type=F32)
     down = down * (1.0 / (1.0 + jnp.exp(-mixv[...])))

time: 65.2 us -> 64.6 us (level); the launches traced: 64.4 us -> 64.5 us
  no operation moved by 1% of the time
where the time goes in v3:
time: 64.6 us; the launch traced here: 64.5 us
  Pallas kernels  61.6 us (95%)
  local copies, waits for them, and re-layouts  2.27 us (4%)
  between operations  0.65 us (1%)
    pallas_call x1, Pallas kernels, per_device(): pl.pallas_call(kernel, out_shape=(jax.ShapeDtypeStruct((ROWS, SL), BF16),...  61.6 us
    unnamed x2, local copies, waits for them, and re-layouts  2.27 us

profile of v3, /device:TPU:2, one launch (start us, length us, event | category | flops | bytes accessed | tf_op | source)
XLA Modules:
  0.0 64.5 jit_solution(17187747919425304354)
XLA Ops:
  0.6 61.6 %layer.1 = (bf16[24,512]{1,0:T(8,128)(2,1)S(1)}, f32[24,2,128,128]{3,2,1,0:T(8,128)S(1)}) custom-call(bf16[24,4096]{1,0:T(8,128)(2,1)} %tok_h.1, f32[24,2,128,128]{3,2,1,0:T(8,128)} %state_h.1, f32[1,4096]{1,0:T(1,128)} %bitcast.18, bf16[128,256]{1,0:T(8,128)(2,1)} %wq_h.1, bf16[128,256]{1,0:T(8,128)(2,1)} %wk_h.1, bf16[128,256]{1,0:T(8,128)(2,1)} %wv_h.1, ...), custom_call_target="tpu_custom_call" | custom-call | tf_op jit(solution)/shard_map/layer/pallas_call | solution.py:519
  62.2 0.6 copy.26
  62.9 1.7 %copy.27 = f32[24,2,128,128]{3,2,1,0:T(8,128)} copy(f32[24,2,128,128]{3,2,1,0:T(8,128)S(1)} %get-tuple-element.5) | data formatting | bytes 6291456

commit v4 on v3

--- a/solution.py
+++ b/solution.py
@@ -17,7 +17,7 @@
 HEAD = 128
 CAP = 3
 SLOTS = NZ * CAP
-N_SEND, N_RECV = 24, 49
+N_SEND, N_RECV = 24, 43
 X_ORDER = (2, 1, 3)
 Z_ORDER = (4, 3, 5, 2, 6, 1, 7)
 Y_ORDER = (2, 1, 3)
@@ -413,19 +413,7 @@
         acc = acc + hidden_part(lax.rem(y + NY - dy, NY) * 2 + other)
 
     def tp_gather(buf):
-        si, rm = new("send"), new("recv")
-        out = [send(buf.at[tp], buf.at[tp], si, new("recv"), at_y(d)) for d in Y_ORDER]
-        send(buf.at[tp], buf.at[tp], si, rm, mate)
-        return si, rm, out
-
-    def tp_hand_on(buf, si, rm, out):
-        for c, d in zip(out, Y_ORDER):
-            c.wait_recv()
-            t = y_index(NY - d)
-            send(buf.at[t], buf.at[t], si, rm, mate)
-        leaves(buf.at[pl.ds(0, NT - 1)], si)
-        got = buf.at[pl.ds(0, NY)]
-        return remote(got, got, ssem.at[si], rsem.at[rm], mate)
+        return exchange(T_ORDER, at_t, lambda d: buf.at[tp], buf.at[tp], buf.at[pl.ds(0, NT - 1)])
 
     c_sc.wait_recv()
     scale = qdst[...].reshape(NX * SLOTS, 128)
@@ -448,8 +436,6 @@
 
     l_ed.wait()
     c_ed.wait_recv()
-    c_eh = tp_hand_on(ehall, *c_eh)
-    c_h = tp_hand_on(hall, *c_h)
     c_eh.wait_recv()
     eres = jnp.zeros((NX * SLOTS, SL), F32)
     for t in range(NT):

time: 64.6 us -> 64.5 us (level)
  no operation moved by 1% of the time
where the time goes in v4:
time: 64.5 us; the launch traced here: 64.2 us
  Pallas kernels  61.3 us (95%)
  local copies, waits for them, and re-layouts  2.27 us (4%)
  between operations  0.65 us (1%)
    pallas_call x1, Pallas kernels, per_device(): pl.pallas_call(kernel, out_shape=(jax.ShapeDtypeStruct((ROWS, SL), BF16),...  61.3 us
    unnamed x2, local copies, waits for them, and re-layouts  2.27 us

profile of v4, /device:TPU:2, one launch (start us, length us, event | category | flops | bytes accessed | tf_op | source)
XLA Modules:
  0.0 64.2 jit_solution(4122370906376088514)
XLA Ops:
  0.6 61.3 %layer.1 = (bf16[24,512]{1,0:T(8,128)(2,1)S(1)}, f32[24,2,128,128]{3,2,1,0:T(8,128)S(1)}) custom-call(bf16[24,4096]{1,0:T(8,128)(2,1)} %tok_h.1, f32[24,2,128,128]{3,2,1,0:T(8,128)} %state_h.1, f32[1,4096]{1,0:T(1,128)} %bitcast.18, bf16[128,256]{1,0:T(8,128)(2,1)} %wq_h.1, bf16[128,256]{1,0:T(8,128)(2,1)} %wk_h.1, bf16[128,256]{1,0:T(8,128)(2,1)} %wv_h.1, ...), custom_call_target="tpu_custom_call" | custom-call | tf_op jit(solution)/shard_map/layer/pallas_call | solution.py:505
  62.0 0.6 copy.26
  62.6 1.7 %copy.27 = f32[24,2,128,128]{3,2,1,0:T(8,128)} copy(f32[24,2,128,128]{3,2,1,0:T(8,128)S(1)} %get-tuple-element.5) | data formatting | bytes 6291456
